TPU v7x, 768 devices: a whole 4x8x12 slice. The times are simulated.
768 devices in a mesh: sp: 96 (over z, y), tp: 8 (over x, core).
Axes of the slice: x: 4, y: 8, z: 12, core: 2. Of those that a mesh axis runs over, the one named last changes fastest.
Arguments:
- proj_value: bfloat16 [49152, 2016], P('sp', 'tp'), may hold values from -6 to 6
- proj_gate: bfloat16 [49152, 2016], P('sp', 'tp'), may hold values from -8 to 8
- conv_saved: bfloat16 [49152, 2016], P('sp', 'tp'), may hold values from -12 to 12
- conv_taps: bfloat16 [31, 2016], P(None, 'tp'), may hold values from -1 to 1
- norm_gain: bfloat16 [2016], P('tp'), may hold values from 0.099609375 to 1.8984375
- out_weight: bfloat16 [2016, 2016], P('tp'), may hold values from -0.125 to 0.125
- cotangent: bfloat16 [49152, 2016], P('sp'), may hold values from -20 to 20
Outputs:
- grad_value: bfloat16 [49152, 2016], P('sp', 'tp')
- grad_gate: bfloat16 [49152, 2016], P('sp', 'tp')
- grad_out_weight: float32 [2016, 2016], P('tp', 'sp')
- grad_taps: float32 [31, 2016], P(None, 'tp')
All inputs are finite; a program needn't handle non-finite values.
Results may differ from a plain program's by a relative error of at most 0.003.
Values sent between devices are 32-bit elements; how exact they have to be, the bound alone decides.
No kernel may reach another device: no remote copies, remote signals or barrier semaphores. Data moves between devices by JAX's collectives and lax.ppermute only.
A program may use at most 32 MiB of HBM per device.

v0:
```python
import functools
import math

import jax
import jax.numpy as jnp
from jax import lax
from jax.experimental import pallas as pl
from jax.experimental.pallas import tpu as pltpu
from jax.sharding import Mesh
from jax.sharding import PartitionSpec as P

SP = ("z", "y")

norm_eps = 1e-05


def from_everyone(x, axis):
    size = lax.axis_size(axis)
    return lax.all_to_all(jnp.broadcast_to(x[None], (size, *x.shape)), axis, 0, 0, tiled=True)


def taken_together(x, axis):
    return from_everyone(x, axis).sum(axis=0)


def shared_rows(a, b, axis):
    return from_everyone(jnp.concatenate([a, b]).reshape(8, -1), axis)


def scattered_sum(x, axes):
    size = lax.axis_size(axes)
    rows, width = x.shape
    each = -(-rows // size)
    padded = jnp.pad(x, ((0, each * size - rows), (0, 0))).reshape(size, each, width)
    return lax.all_to_all(padded, axes, 0, 0, tiled=True).sum(axis=0)


def passed_along(block, axis, distance):
    devices = range(lax.axis_size(axis))
    route = [(i - distance, i) for i in devices if i - distance in devices]
    return lax.ppermute(block, axis, route)


def column(lanes, rows):
    turned = lanes.T
    return jnp.concatenate([turned[:, r : r + 1] for r in rows], axis=0)


def weight_grad_kernel(model_width, groups, shared_ref, conv_ref, gain_ref, cot_ref, out_ref, act_ref):
    totals = jnp.sum(shared_ref[...], axis=0) / model_width
    mean = column(totals, range(4))
    square = column(totals, range(4, 8))
    inv_std = lax.rsqrt(square - mean * mean + norm_eps)
    centered = (conv_ref[...].astype(jnp.float32) - mean) * inv_std
    normed = centered * gain_ref[...].astype(jnp.float32)
    act_ref[...] = (normed * jax.nn.sigmoid(normed)).astype(jnp.bfloat16)
    inner, each = out_ref.shape[0], out_ref.shape[2]
    block = groups * inner * each

    def one(i, carry):
        rows = pl.ds(pl.multiple_of(i * block, block), block)
        res = jnp.dot(cot_ref[rows, :], act_ref[...], preferred_element_type=jnp.float32)
        for g in range(groups):
            for y in range(inner):
                at = (g * inner + y) * each
                out_ref[y, i * groups + g] = res[at : at + each]
        return carry

    lax.fori_loop(0, cot_ref.shape[0] // block, one, 0)


def weight_grad(shared, conv_saved, gain, cot_t, outer, inner):
    model_width, width = cot_t.shape[0], conv_saved.shape[1]
    each = model_width // (outer * inner)
    return pl.pallas_call(
        functools.partial(weight_grad_kernel, model_width, 2),
        out_shape=jax.ShapeDtypeStruct((inner, outer, each, width), jnp.float32),
        scratch_shapes=[pltpu.VMEM(conv_saved.shape, jnp.bfloat16)],
        cost_estimate=pl.CostEstimate(
            flops=2 * conv_saved.size * model_width,
            bytes_accessed=2 * cot_t.size + 4 * model_width * width,
            transcendentals=conv_saved.size,
        ),
        compiler_params=pltpu.CompilerParams(vmem_limit_bytes=16 * 2**20),
        name="weight_grad",
    )(shared, conv_saved, gain, cot_t)


STEP = 32


def filter_rows(window, value, gate, taps_ref, tap_sums_ref):
    tap_count = taps_ref.shape[0]
    gate_proj = jax.nn.sigmoid(gate.astype(jnp.float32))
    gated = value.astype(jnp.float32) * gate_proj
    d_glu = jnp.zeros_like(gated)
    for phase in range(8):
        turned = window[phase : phase + 2 * STEP - 8]
        for at in range(phase, tap_count, 8):
            k = tap_count - 1 - at
            shifted = turned[at - phase : at - phase + STEP]
            d_glu += taps_ref[k : k + 1].astype(jnp.float32) * shifted
            tap_sums_ref[k] += (gated * shifted).reshape(STEP // 8, 8, -1).sum(axis=0)
    grad_value = d_glu * gate_proj
    grad_gate = d_glu * gated * (1.0 - gate_proj)
    return grad_value.astype(jnp.bfloat16), grad_gate.astype(jnp.bfloat16)


def main_rows_kernel(conv_grad_ref, value_ref, gate_ref, taps_ref, value_out, gate_out, tap_out):
    tap_out[...] = jnp.zeros_like(tap_out)

    def one(i, carry):
        at = pl.multiple_of(i * STEP, STEP)
        rows = pl.ds(at, STEP)
        value_out[rows], gate_out[rows] = filter_rows(
            conv_grad_ref[pl.ds(at, 2 * STEP)], value_ref[rows], gate_ref[rows], taps_ref, tap_out
        )
        return carry

    lax.fori_loop(0, value_ref.shape[0] // STEP - 1, one, 0)
    last = value_ref.shape[0] - STEP
    value_out[last:] = jnp.zeros((STEP, value_out.shape[1]), value_out.dtype)
    gate_out[last:] = jnp.zeros((STEP, gate_out.shape[1]), gate_out.dtype)


def last_rows_kernel(
    conv_grad_ref, ahead_ref, value_ref, gate_ref, taps_ref, value_in, gate_in, tap_in, value_out, gate_out, tap_out, sums_ref
):
    last = value_ref.shape[0] - STEP
    width = conv_grad_ref.shape[1]
    ahead = ahead_ref[...]
    fill = jnp.zeros((STEP - ahead.shape[0], width), jnp.float32)
    window = jnp.concatenate([conv_grad_ref[last:], ahead, fill], axis=0)
    sums_ref[...] = tap_in[...]
    value_out[:last] = value_in[:last]
    gate_out[:last] = gate_in[:last]
    value_out[last:], gate_out[last:] = filter_rows(window, value_ref[last:], gate_ref[last:], taps_ref, sums_ref)
    tap_count = taps_ref.shape[0]
    tap_out[:tap_count] = jnp.sum(sums_ref[...], axis=1)
    tap_out[tap_count:] = jnp.zeros((tap_out.shape[0] - tap_count, width), jnp.float32)


def main_rows(conv_grad, value, gate, taps):
    grad = jax.ShapeDtypeStruct(value.shape, jnp.bfloat16)
    return pl.pallas_call(
        main_rows_kernel,
        out_shape=(grad, grad, jax.ShapeDtypeStruct((taps.shape[0], 8, taps.shape[1]), jnp.float32)),
        cost_estimate=pl.CostEstimate(flops=4 * taps.shape[0] * value.size, bytes_accessed=12 * value.size, transcendentals=value.size),
        compiler_params=pltpu.CompilerParams(vmem_limit_bytes=12 * 2**20),
        name="main_rows",
    )(conv_grad, value, gate, taps)


def last_rows(conv_grad, ahead, value, gate, taps, done, padded_taps):
    grad = jax.ShapeDtypeStruct(value.shape, jnp.bfloat16)
    return pl.pallas_call(
        last_rows_kernel,
        out_shape=(grad, grad, jax.ShapeDtypeStruct((padded_taps, taps.shape[1]), jnp.float32)),
        scratch_shapes=[pltpu.VMEM(done[2].shape, jnp.float32)],
        cost_estimate=pl.CostEstimate(flops=4 * taps.size * STEP, bytes_accessed=16 * value.size, transcendentals=0),
        compiler_params=pltpu.CompilerParams(vmem_limit_bytes=12 * 2**20),
        name="last_rows",
    )(conv_grad, ahead, value, gate, taps, *done)


def local(proj_value, proj_gate, conv_saved, conv_taps, norm_gain, out_weight, cotangent):
    model_width = cotangent.shape[1]
    tok_rows = cotangent.shape[0]
    tap_count = conv_taps.shape[0]
    overhang = tap_count - 1
    grad_scale = 1.0 / math.sqrt(tok_rows * lax.axis_size(SP))
    z_size, y_size = (lax.axis_size(a) for a in SP)
    d_act = lax.dot_general(
        cotangent, out_weight, (((1,), (1,)), ((), ())), preferred_element_type=jnp.float32
    )
    conv_f = conv_saved.astype(jnp.float32)
    shared = shared_rows(jnp.sum(conv_f, axis=1), jnp.sum(conv_f * conv_f, axis=1), "tp")
    shared, d_act = lax.optimization_barrier((shared, d_act))
    terms = weight_grad(shared, conv_saved, norm_gain[None], cotangent.T, z_size, y_size)
    terms = lax.psum_scatter(terms, "y", scatter_dimension=0)
    totals = shared.sum(axis=0).reshape(2, tok_rows)
    row_mean = totals[0] / model_width
    row_var = totals[1] / model_width - row_mean * row_mean
    inv_std = lax.rsqrt(row_var + norm_eps)
    centered = (conv_f - row_mean[:, None]) * inv_std[:, None]
    gain_f = norm_gain.astype(jnp.float32)
    normed = centered * gain_f
    gate_norm = jax.nn.sigmoid(normed)
    d_hat = d_act * gate_norm * (1.0 + normed * (1.0 - gate_norm)) * gain_f
    moments = shared_rows(jnp.sum(d_hat, axis=1), jnp.sum(d_hat * centered, axis=1), "tp")
    moments = moments.sum(axis=0).reshape(2, tok_rows)
    first = moments[0] / model_width
    second = moments[1] / model_width
    d_conv = inv_std[:, None] * (d_hat - first[:, None] - centered * second[:, None])
    ahead = passed_along(d_conv[:overhang], SP, -1)
    done = main_rows(d_conv, proj_value, proj_gate, conv_taps)
    padded_taps = -(-tap_count // z_size) * z_size
    grad_value, grad_gate, tap_sums = last_rows(d_conv, ahead, proj_value, proj_gate, conv_taps, done, padded_taps)
    tap_part = taken_together(scattered_sum(tap_sums, "z"), "y")
    each = terms.shape[1]
    spread = jnp.broadcast_to(tap_part[None], (z_size, *tap_part.shape))
    arrived = lax.all_to_all(jnp.concatenate([terms, spread], axis=1), "z", 0, 0, tiled=True)
    grad_out_weight = arrived[:, :each].sum(axis=0).T * grad_scale
    grad_taps = arrived[:, each:].reshape(-1, arrived.shape[2])[:tap_count] * grad_scale
    return (grad_value, grad_gate, grad_out_weight, grad_taps)


def solution(mesh):
    split = Mesh(mesh.devices.reshape(12, 8, mesh.shape["tp"]), (*SP, "tp"))
    return jax.shard_map(
        local,
        mesh=split,
        in_specs=(
            P(SP, "tp"),
            P(SP, "tp"),
            P(SP, "tp"),
            P(None, "tp"),
            P("tp"),
            P("tp", None),
            P(SP, None),
        ),
        out_specs=(P(SP, "tp"), P(SP, "tp"), P("tp", SP), P(None, "tp")),
        check_vma=False,
    )
```

profile of v0, /device:TPU:24, one launch (start us, length us, event | category | flops | bytes accessed | tf_op | source)
XLA Modules:
  0.0 109.4 jit_solution(16344398241075535654)
XLA Ops:
  7.2 0.0 copy-start
  7.2 0.0 copy-start.2
  7.2 0.0 copy-start.1
  7.2 0.0 copy-start.7
  7.2 1.3 %convert_reduce_fusion = (f32[512]{0:T(512)S(1)}, f32[512]{0:T(512)S(1)}) fusion(bf16[512,252]{1,0:T(8,128)(2,1)} %conv_ref.1), kind=kLoop, calls=%fused_computation.2 | loop fusion | flops 515072 | bytes 262144 | tf_op jit(solution)/shard_map/reduce_sum | solution.py:177
  8.6 0.6 broadcast_in_dim.10
  9.2 4.3 %all-to-all-start = ((f32[8,8,128]{2,1,0:T(8,128)}), f32[8,8,128]{2,1,0:T(8,128)S(1)}, u32[]{:S(2)}, u32[]{:S(2)}) async-start(f32[8,8,128]{2,1,0:T(8,128)} %broadcast_in_dim.10), calls=%async_computation | async-start | bytes 65536 | tf_op jit(solution)/shard_map/all_to_all | solution.py:19
  13.5 0.0 reduce-scatter.2.cloned.1.call-start
  13.5 0.0 copy-done
  13.5 3.1 %fusion.20 = f32[512,252]{1,0:T(8,128)} fusion(bf16[512,2016]{0,1:T(8,128)(2,1)} %param.13, bf16[252,2016]{0,1:T(8,128)(2,1)S(1)} %copy-done), kind=kOutput, calls=%fused_computation.32 | convolution fusion | flops 520224768 | bytes 3596544 | tf_op jit(solution)/shard_map/dot_general | solution.py:173
  16.7 0.0 copy-done.7
  16.7 2.2 %all-to-all-done.shared_ref = f32[8,8,128]{2,1,0:T(8,128)S(1)} async-done(((f32[8,8,128]{2,1,0:T(8,128)}), f32[8,8,128]{2,1,0:T(8,128)S(1)}, u32[]{:S(2)}, u32[]{:S(2)}) %all-to-all-start) | async-done | bytes 32800 | tf_op jit(solution)/shard_map/all_to_all | solution.py:19
  18.9 0.0 copy-done.2
  18.9 0.0 copy-done.1
  18.9 3.4 %weight_grad.1 = f32[8,12,21,252]{3,2,1,0:T(8,128)} custom-call(f32[8,8,128]{2,1,0:T(8,128)S(1)} %all-to-all-done.shared_ref, bf16[512,252]{1,0:T(8,128)(2,1)S(1)} %copy-done.2, bf16[1,252]{1,0:T(2,128)(2,1)S(1)} %broadcast_in_dim.12.gain_ref, bf16[2016,512]{1,0:T(8,128)(2,1)S(1)} %bitcast.24), custom_call_target="tpu_custom_call" | custom-call | flops 520224768 | bytes 4096512 | tf_op jit(solution)/shard_map/weight_grad/pallas_call | solution.py:75
  22.4 0.0 reduce-scatter.2.cloned.1.call-update
  22.4 1.0 copy-done.6
  23.4 0.5 fusion.18
  23.9 7.8 %all_to_all.25 = f32[8,8,128]{2,1,0:T(8,128)S(1)} all-to-all(f32[8,8,128]{2,1,0:T(8,128)S(1)} %broadcast_in_dim.11), channel_id=1, replica_groups=mesh['z'=12,'y'=8,'tp'=8] {'tp'}, dimensions={0} | all-to-all | bytes 65536 | tf_op jit(solution)/shard_map/all_to_all | solution.py:19
  31.8 0.3 fusion.15.conv_grad_ref
  32.1 2.4 %collective-permute-start = (f32[30,252]{1,0:T(8,128)S(1)}, f32[30,252]{1,0:T(8,128)S(1)}, u32[]{:S(2)}, u32[]{:S(2)}) collective-permute-start(f32[30,252]{1,0:T(8,128)S(1)} %slice.36), channel_id=1, source_target_pairs={{8,0},{16,8},{24,16},{32,24},{40,32},{48,40},{56,48},{64,56},{72,6... | collective-permute-start | bytes 90728 | tf_op jit(solution)/shard_map/ppermute | solution.py:41
  34.5 0.0 copy-done.3
  34.5 4.6 %main_rows.1 = (bf16[512,252]{1,0:T(8,128)(2,1)S(1)}, bf16[512,252]{1,0:T(8,128)(2,1)S(1)}, f32[31,8,252]{2,1,0:T(8,128)S(1)}) custom-call(f32[512,252]{1,0:T(8,128)S(1)} %fusion.15.conv_grad_ref, bf16[512,252]{1,0:T(8,128)(2,1)S(1)} %copy-done.3, bf16[512,252]{1,0:T(8,128)(2,1)S(1)} %copy-done.4, bf16[31,252]{1,0:T(8,128)(2,1)S(1)} %copy-done.5), custom_call_target="tpu_custom_call" | custom-call | flops 15998976 | bytes 1548288 | tf_op jit(solution)/shard_map/main_rows/pallas_call | solution.py:145
  39.1 0.0 collective-permute-done.ahead_ref
  39.1 1.1 %last_rows.1 = (bf16[512,252]{1,0:T(8,128)(2,1)}, bf16[512,252]{1,0:T(8,128)(2,1)}, f32[36,252]{1,0:T(8,128)S(1)}) custom-call(f32[512,252]{1,0:T(8,128)S(1)} %fusion.15.conv_grad_ref, f32[30,252]{1,0:T(8,128)S(1)} %collective-permute-done.ahead_ref, bf16[512,252]{1,0:T(8,128)(2,1)S(1)} %copy-done.3, bf16[512,252]{1,0:T(8,128)(2,1)S(1)} %copy-done.4, ...), custom_call_target="tpu_custom_call" | custom-call | flops 999936 | bytes 2064384 | tf_op jit(solution)/shard_map/last_rows/pallas_call | solution.py:156
  40.3 25.8 %all_to_all.26 = f32[12,3,252]{2,1,0:T(4,128)S(1)} all-to-all(f32[12,3,252]{2,1,0:T(4,128)S(1)} %reshape.68), channel_id=1, replica_groups=mesh['z'=12,'y'=8,'tp'=8] {'z'}, dimensions={0} | all-to-all | bytes 72576 | tf_op jit(solution)/shard_map/all_to_all | solution.py:35
  66.1 12.0 %all_to_all.27 = f32[8,3,252]{2,1,0:T(4,128)S(1)} all-to-all(f32[8,3,252]{2,1,0:T(4,128)S(1)} %broadcast_in_dim.13), channel_id=1, replica_groups=mesh['z'=12,'y'=8,'tp'=8] {'y'}, dimensions={0} | all-to-all | bytes 48384 | tf_op jit(solution)/shard_map/all_to_all | solution.py:19
  78.1 0.0 reduce-scatter.2.cloned.1.call-done
  78.2 1.0 pad_maximum_fusion
  79.2 22.1 %all_to_all.28 = f32[12,24,252]{2,1,0:T(8,128)S(1)} all-to-all(f32[12,24,252]{2,1,0:T(8,128)S(1)} %pad_maximum_fusion), channel_id=1, replica_groups=mesh['z'=12,'y'=8,'tp'=8] {'z'}, dimensions={0} | all-to-all | bytes 580608 | tf_op jit(solution)/shard_map/all_to_all | solution.py:202
  101.3 0.6 slice_multiply_fusion
  102.0 0.6 multiply_bitcast_fusion
  (25 shorter events, 0.2 us)
Async XLA Ops:
  7.2 6.4 %copy-start = (bf16[252,2016]{0,1:T(8,128)(2,1)S(1)}, bf16[252,2016]{0,1:T(8,128)(2,1)}, u32[]{:S(2)}) copy-start(bf16[252,2016]{0,1:T(8,128)(2,1)} %param.12) | copy-start | bytes 3048196
  7.2 11.7 %copy-start.2 = (bf16[512,252]{1,0:T(8,128)(2,1)S(1)}, bf16[512,252]{1,0:T(8,128)(2,1)}, u32[]{:S(2)}) copy-start(bf16[512,252]{1,0:T(8,128)(2,1)} %conv_ref.1) | copy-start | bytes 774148
  7.2 11.7 %copy-start.1 = (bf16[512,2016]{0,1:T(8,128)(2,1)S(1)}, bf16[512,2016]{0,1:T(8,128)(2,1)}, u32[]{:S(2)}) copy-start(bf16[512,2016]{0,1:T(8,128)(2,1)} %param.13) | copy-start | bytes 6193156
  7.2 9.5 %copy-start.7 = (bf16[252]{0:T(256)(128)(2,1)S(1)}, bf16[252]{0:T(256)(128)(2,1)}, u32[]{:S(2)}) copy-start(bf16[252]{0:T(256)(128)(2,1)} %param.11) | copy-start | bytes 1516
  9.2 9.7 %all-to-all-start = ((f32[8,8,128]{2,1,0:T(8,128)}), f32[8,8,128]{2,1,0:T(8,128)S(1)}, u32[]{:S(2)}, u32[]{:S(2)}) async-start(f32[8,8,128]{2,1,0:T(8,128)} %broadcast_in_dim.10), calls=%async_computation | async-start | bytes 65536 | tf_op jit(solution)/shard_map/all_to_all | solution.py:19
  13.5 64.7 %reduce-scatter.2.cloned.1.call-start = ((), (), s32[]{:S(2)}) async-start(), calls=%async_computation.6 | async-start | bytes 2654208 | tf_op jit(solution)/shard_map/reduce_scatter | solution.py:180
  22.3 1.0 copy-start.6
  22.3 12.1 %copy-start.3 = (bf16[512,252]{1,0:T(8,128)(2,1)S(1)}, bf16[512,252]{1,0:T(8,128)(2,1)}, u32[]{:S(2)}) copy-start(bf16[512,252]{1,0:T(8,128)(2,1)} %value_ref.3) | copy-start | bytes 774148
  22.3 12.1 %copy-start.4 = (bf16[512,252]{1,0:T(8,128)(2,1)S(1)}, bf16[512,252]{1,0:T(8,128)(2,1)}, u32[]{:S(2)}) copy-start(bf16[512,252]{1,0:T(8,128)(2,1)} %gate_ref.3) | copy-start | bytes 774148
  22.4 12.1 %copy-start.5 = (bf16[31,252]{1,0:T(8,128)(2,1)S(1)}, bf16[31,252]{1,0:T(8,128)(2,1)}, u32[]{:S(2)}) copy-start(bf16[31,252]{1,0:T(8,128)(2,1)} %taps_ref.3) | copy-start | bytes 46876
  32.1 7.0 %collective-permute-start = (f32[30,252]{1,0:T(8,128)S(1)}, f32[30,252]{1,0:T(8,128)S(1)}, u32[]{:S(2)}, u32[]{:S(2)}) collective-permute-start(f32[30,252]{1,0:T(8,128)S(1)} %slice.36), channel_id=1, source_target_pairs={{8,0},{16,8},{24,16},{32,24},{40,32},{48,40},{56,48},{64,56},{72,6... | collective-permute-start | bytes 90728 | tf_op jit(solution)/shard_map/ppermute | solution.py:41
Sparse Core Ops, SparseCore 0:
  22.5 52.7 reduce-scatter.1
where the time goes:
time: 110 us; the launch traced here: 109 us
  blocking collectives  67.7 us (62%)
  between operations  14.2 us (13%)
  Pallas kernels  9.15 us (8%)
  starting transfers between devices  6.69 us (6%)
  other arithmetic  4.54 us (4%)
  matrix products  3.14 us (3%)
  waiting for transfers between devices  2.3 us (2%)
  local copies, waits for them, and re-layouts  1.69 us (2%)
    all_to_all x1, blocking collectives, scattered_sum(): return lax.all_to_all(padded, axes, 0, 0, tiled=True).sum(axis=0)  25.8 us
    all_to_all x1, blocking collectives, local(): lax.all_to_all(jnp.concatenate([terms, spread], axis=1), 'z', 0, 0, tiled...  22.1 us
    all_to_all x2, blocking collectives, from_everyone(): lax.all_to_all(jnp.broadcast_to(x[None], (size, *x.shape)), axis, 0, 0, t...  19.8 us
    pallas_call x1, Pallas kernels, main_rows(): pl.pallas_call(main_rows_kernel, out_shape=(grad, grad, jax.ShapeDtypeStr...  4.61 us
    all_to_all x1, starting transfers between devices, from_everyone(): lax.all_to_all(jnp.broadcast_to(x[None], (size, *x.shape)), axis, 0, 0, t...  4.3 us
    pallas_call x1, Pallas kernels, weight_grad(): pl.pallas_call(functools.partial(weight_grad_kernel, model_width, 2), out...  3.41 us
    dot_general x1, matrix products, local(): lax.dot_general(cotangent, out_weight, (((1,), (1,)), ((), ())), preferre...  3.14 us
    ppermute x1, starting transfers between devices, passed_along(): return lax.ppermute(block, axis, route)  2.36 us
  transfers between devices with their start and end apart: 3, of which 1 were waited for; matrix products, arithmetic and copies ran while one was open for 4% of the time, Pallas kernels for 5%

commit v1 on v0

--- a/solution.py
+++ b/solution.py
@@ -23,10 +23,6 @@
     return from_everyone(x, axis).sum(axis=0)
 
 
-def shared_rows(a, b, axis):
-    return from_everyone(jnp.concatenate([a, b]).reshape(8, -1), axis)
-
-
 def scattered_sum(x, axes):
     size = lax.axis_size(axes)
     rows, width = x.shape
@@ -46,35 +42,79 @@
     return jnp.concatenate([turned[:, r : r + 1] for r in rows], axis=0)
 
 
-def weight_grad_kernel(model_width, groups, shared_ref, conv_ref, gain_ref, cot_ref, out_ref, act_ref):
+def spread_rows(first, second, out_ref):
+    columns = [c[at : at + 128] for c in (first, second) for at in range(0, c.shape[0], 128)]
+    rows = jnp.concatenate(columns, axis=1).T
+    for i in range(out_ref.shape[0]):
+        out_ref[i] = rows
+
+
+def statistics_kernel(conv_ref, out_ref):
+    conv = conv_ref[...].astype(jnp.float32)
+    spread_rows(jnp.sum(conv, axis=1, keepdims=True), jnp.sum(conv * conv, axis=1, keepdims=True), out_ref)
+
+
+def statistics(conv_saved, devices):
+    return pl.pallas_call(
+        statistics_kernel,
+        out_shape=jax.ShapeDtypeStruct((devices, conv_saved.shape[0] // 64, 128), jnp.float32),
+        cost_estimate=pl.CostEstimate(flops=3 * conv_saved.size, bytes_accessed=2 * conv_saved.size, transcendentals=0),
+        compiler_params=pltpu.CompilerParams(vmem_limit_bytes=8 * 2**20),
+        name="statistics",
+    )(conv_saved)
+
+
+def standardized(model_width, shared_ref, conv_ref):
     totals = jnp.sum(shared_ref[...], axis=0) / model_width
-    mean = column(totals, range(4))
-    square = column(totals, range(4, 8))
+    half = totals.shape[0] // 2
+    mean = column(totals, range(half))
+    square = column(totals, range(half, 2 * half))
     inv_std = lax.rsqrt(square - mean * mean + norm_eps)
-    centered = (conv_ref[...].astype(jnp.float32) - mean) * inv_std
+    return (conv_ref[...].astype(jnp.float32) - mean) * inv_std
+
+
+def norm_grad_kernel(model_width, shared_ref, conv_ref, gain_ref, act_grad_ref, hat_ref, out_ref):
+    centered = standardized(model_width, shared_ref, conv_ref)
+    gain = gain_ref[...].astype(jnp.float32)
+    normed = centered * gain
+    gate_norm = jax.nn.sigmoid(normed)
+    d_hat = act_grad_ref[...] * gate_norm * (1.0 + normed * (1.0 - gate_norm)) * gain
+    hat_ref[...] = d_hat
+    spread_rows(jnp.sum(d_hat, axis=1, keepdims=True), jnp.sum(d_hat * centered, axis=1, keepdims=True), out_ref)
+
+
+def norm_grad(model_width, shared, conv_saved, gain, act_grad):
+    return pl.pallas_call(
+        functools.partial(norm_grad_kernel, model_width),
+        out_shape=(jax.ShapeDtypeStruct(conv_saved.shape, jnp.float32), jax.ShapeDtypeStruct(shared.shape, jnp.float32)),
+        cost_estimate=pl.CostEstimate(
+            flops=20 * conv_saved.size, bytes_accessed=10 * conv_saved.size, transcendentals=conv_saved.size
+        ),
+        compiler_params=pltpu.CompilerParams(vmem_limit_bytes=8 * 2**20),
+        name="norm_grad",
+    )(shared, conv_saved, gain, act_grad)
+
+
+def weight_grad_kernel(model_width, z_size, shared_ref, conv_ref, gain_ref, cot_ref, out_ref, act_ref):
+    centered = standardized(model_width, shared_ref, conv_ref)
     normed = centered * gain_ref[...].astype(jnp.float32)
     act_ref[...] = (normed * jax.nn.sigmoid(normed)).astype(jnp.bfloat16)
-    inner, each = out_ref.shape[0], out_ref.shape[2]
-    block = groups * inner * each
-
-    def one(i, carry):
-        rows = pl.ds(pl.multiple_of(i * block, block), block)
-        res = jnp.dot(cot_ref[rows, :], act_ref[...], preferred_element_type=jnp.float32)
-        for g in range(groups):
-            for y in range(inner):
-                at = (g * inner + y) * each
-                out_ref[y, i * groups + g] = res[at : at + each]
-        return carry
-
-    lax.fori_loop(0, cot_ref.shape[0] // block, one, 0)
-
-
-def weight_grad(shared, conv_saved, gain, cot_t, outer, inner):
+    y_size = out_ref.shape[0]
+    each = out_ref.shape[1] // z_size
+    block = 2 * y_size * each
+    for i in range(z_size // 2):
+        res = jnp.dot(cot_ref[i * block : (i + 1) * block], act_ref[...], preferred_element_type=jnp.float32)
+        for g in range(2):
+            for y in range(y_size):
+                at, to = (g * y_size + y) * each, (2 * i + g) * each
+                out_ref[y, to : to + each] = res[at : at + each]
+
+
+def weight_grad(shared, conv_saved, gain, cot_t, z_size, y_size):
     model_width, width = cot_t.shape[0], conv_saved.shape[1]
-    each = model_width // (outer * inner)
-    return pl.pallas_call(
-        functools.partial(weight_grad_kernel, model_width, 2),
-        out_shape=jax.ShapeDtypeStruct((inner, outer, each, width), jnp.float32),
+    return pl.pallas_call(
+        functools.partial(weight_grad_kernel, model_width, z_size),
+        out_shape=jax.ShapeDtypeStruct((y_size, model_width // y_size, width), jnp.float32),
         scratch_shapes=[pltpu.VMEM(conv_saved.shape, jnp.bfloat16)],
         cost_estimate=pl.CostEstimate(
             flops=2 * conv_saved.size * model_width,
@@ -89,31 +129,40 @@
 STEP = 32
 
 
-def filter_rows(window, value, gate, taps_ref, tap_sums_ref):
-    tap_count = taps_ref.shape[0]
+def widen(taps_ref, wide_ref):
+    for k in range(taps_ref.shape[0]):
+        wide_ref[k] = jnp.broadcast_to(taps_ref[k : k + 1].astype(jnp.float32), wide_ref.shape[1:])
+
+
+def filter_rows(window, value, gate, wide_ref, tap_sums_ref):
+    tap_count = wide_ref.shape[0]
     gate_proj = jax.nn.sigmoid(gate.astype(jnp.float32))
     gated = value.astype(jnp.float32) * gate_proj
-    d_glu = jnp.zeros_like(gated)
+    groups = (STEP // 8, 8, gated.shape[1])
+    gated_groups = gated.reshape(groups)
+    d_glu = jnp.zeros(groups, jnp.float32)
     for phase in range(8):
         turned = window[phase : phase + 2 * STEP - 8]
         for at in range(phase, tap_count, 8):
             k = tap_count - 1 - at
-            shifted = turned[at - phase : at - phase + STEP]
-            d_glu += taps_ref[k : k + 1].astype(jnp.float32) * shifted
-            tap_sums_ref[k] += (gated * shifted).reshape(STEP // 8, 8, -1).sum(axis=0)
+            shifted = turned[at - phase : at - phase + STEP].reshape(groups)
+            d_glu += wide_ref[k] * shifted
+            tap_sums_ref[k] += (gated_groups * shifted).sum(axis=0)
+    d_glu = d_glu.reshape(gated.shape)
     grad_value = d_glu * gate_proj
     grad_gate = d_glu * gated * (1.0 - gate_proj)
     return grad_value.astype(jnp.bfloat16), grad_gate.astype(jnp.bfloat16)
 
 
-def main_rows_kernel(conv_grad_ref, value_ref, gate_ref, taps_ref, value_out, gate_out, tap_out):
+def main_rows_kernel(conv_grad_ref, value_ref, gate_ref, taps_ref, value_out, gate_out, tap_out, wide_ref):
     tap_out[...] = jnp.zeros_like(tap_out)
+    widen(taps_ref, wide_ref)
 
     def one(i, carry):
         at = pl.multiple_of(i * STEP, STEP)
         rows = pl.ds(at, STEP)
         value_out[rows], gate_out[rows] = filter_rows(
-            conv_grad_ref[pl.ds(at, 2 * STEP)], value_ref[rows], gate_ref[rows], taps_ref, tap_out
+            conv_grad_ref[pl.ds(at, 2 * STEP)], value_ref[rows], gate_ref[rows], wide_ref, tap_out
         )
         return carry
 
@@ -124,7 +173,7 @@
 
 
 def last_rows_kernel(
-    conv_grad_ref, ahead_ref, value_ref, gate_ref, taps_ref, value_in, gate_in, tap_in, value_out, gate_out, tap_out, sums_ref
+    conv_grad_ref, ahead_ref, value_ref, gate_ref, taps_ref, value_in, gate_in, tap_in, value_out, gate_out, tap_out, sums_ref, wide_ref
 ):
     last = value_ref.shape[0] - STEP
     width = conv_grad_ref.shape[1]
@@ -132,9 +181,10 @@
     fill = jnp.zeros((STEP - ahead.shape[0], width), jnp.float32)
     window = jnp.concatenate([conv_grad_ref[last:], ahead, fill], axis=0)
     sums_ref[...] = tap_in[...]
+    widen(taps_ref, wide_ref)
     value_out[:last] = value_in[:last]
     gate_out[:last] = gate_in[:last]
-    value_out[last:], gate_out[last:] = filter_rows(window, value_ref[last:], gate_ref[last:], taps_ref, sums_ref)
+    value_out[last:], gate_out[last:] = filter_rows(window, value_ref[last:], gate_ref[last:], wide_ref, sums_ref)
     tap_count = taps_ref.shape[0]
     tap_out[:tap_count] = jnp.sum(sums_ref[...], axis=1)
     tap_out[tap_count:] = jnp.zeros((tap_out.shape[0] - tap_count, width), jnp.float32)
@@ -145,6 +195,7 @@
     return pl.pallas_call(
         main_rows_kernel,
         out_shape=(grad, grad, jax.ShapeDtypeStruct((taps.shape[0], 8, taps.shape[1]), jnp.float32)),
+        scratch_shapes=[pltpu.VMEM((taps.shape[0], 8, taps.shape[1]), jnp.float32)],
         cost_estimate=pl.CostEstimate(flops=4 * taps.shape[0] * value.size, bytes_accessed=12 * value.size, transcendentals=value.size),
         compiler_params=pltpu.CompilerParams(vmem_limit_bytes=12 * 2**20),
         name="main_rows",
@@ -156,7 +207,7 @@
     return pl.pallas_call(
         last_rows_kernel,
         out_shape=(grad, grad, jax.ShapeDtypeStruct((padded_taps, taps.shape[1]), jnp.float32)),
-        scratch_shapes=[pltpu.VMEM(done[2].shape, jnp.float32)],
+        scratch_shapes=[pltpu.VMEM(done[2].shape, jnp.float32)] * 2,
         cost_estimate=pl.CostEstimate(flops=4 * taps.size * STEP, bytes_accessed=16 * value.size, transcendentals=0),
         compiler_params=pltpu.CompilerParams(vmem_limit_bytes=12 * 2**20),
         name="last_rows",
@@ -173,21 +224,19 @@
     d_act = lax.dot_general(
         cotangent, out_weight, (((1,), (1,)), ((), ())), preferred_element_type=jnp.float32
     )
-    conv_f = conv_saved.astype(jnp.float32)
-    shared = shared_rows(jnp.sum(conv_f, axis=1), jnp.sum(conv_f * conv_f, axis=1), "tp")
+    everyone = lambda x: lax.all_to_all(x, "tp", 0, 0, tiled=True)
+    shared = everyone(statistics(conv_saved, lax.axis_size("tp")))
     shared, d_act = lax.optimization_barrier((shared, d_act))
     terms = weight_grad(shared, conv_saved, norm_gain[None], cotangent.T, z_size, y_size)
     terms = lax.psum_scatter(terms, "y", scatter_dimension=0)
+    terms = terms.reshape(z_size, -1, terms.shape[1])
+    d_hat, moments = norm_grad(model_width, shared, conv_saved, norm_gain[None], d_act)
+    moments = everyone(moments)
     totals = shared.sum(axis=0).reshape(2, tok_rows)
     row_mean = totals[0] / model_width
     row_var = totals[1] / model_width - row_mean * row_mean
     inv_std = lax.rsqrt(row_var + norm_eps)
-    centered = (conv_f - row_mean[:, None]) * inv_std[:, None]
-    gain_f = norm_gain.astype(jnp.float32)
-    normed = centered * gain_f
-    gate_norm = jax.nn.sigmoid(normed)
-    d_hat = d_act * gate_norm * (1.0 + normed * (1.0 - gate_norm)) * gain_f
-    moments = shared_rows(jnp.sum(d_hat, axis=1), jnp.sum(d_hat * centered, axis=1), "tp")
+    centered = (conv_saved.astype(jnp.float32) - row_mean[:, None]) * inv_std[:, None]
     moments = moments.sum(axis=0).reshape(2, tok_rows)
     first = moments[0] / model_width
     second = moments[1] / model_width

time: 110 us -> 108 us (0.982)
  the two profiles are of different devices: /device:TPU:24 before, /device:TPU:4 now
where the time goes in v1:
time: 108 us
  blocking collectives  52.5 us (49%)
  starting transfers between devices  19.6 us (18%)
  between operations  14.2 us (13%)
  Pallas kernels  8.73 us (8%)
  waiting for transfers between devices  4.6 us (4%)
  local copies, waits for them, and re-layouts  3.18 us (3%)
  matrix products  3.13 us (3%)
  other arithmetic  1.72 us (2%)
    all_to_all x1, blocking collectives, scattered_sum(): return lax.all_to_all(padded, axes, 0, 0, tiled=True).sum(axis=0)  20.4 us
    all_to_all x1, blocking collectives, local(): lax.all_to_all(jnp.concatenate([terms, spread], axis=1), 'z', 0, 0, tiled...  18.8 us
    all_to_all x2, starting transfers between devices, local(): everyone = lambda x: lax.all_to_all(x, 'tp', 0, 0, tiled=True)  18.3 us
    all_to_all x1, blocking collectives, from_everyone(): lax.all_to_all(jnp.broadcast_to(x[None], (size, *x.shape)), axis, 0, 0, t...  13.4 us
    dot_general x1, matrix products, local(): lax.dot_general(cotangent, out_weight, (((1,), (1,)), ((), ())), preferre...  3.13 us
    all_to_all x2, waiting for transfers between devices, local(): everyone = lambda x: lax.all_to_all(x, 'tp', 0, 0, tiled=True)  3.01 us
    pallas_call x1, Pallas kernels, main_rows(): pl.pallas_call(main_rows_kernel, out_shape=(grad, grad, jax.ShapeDtypeStr...  2.91 us
    pallas_call x1, Pallas kernels, weight_grad(): pl.pallas_call(functools.partial(weight_grad_kernel, model_width, z_size)...  2.53 us
  transfers between devices with their start and end apart: 4, of which 2 were waited for; matrix products, arithmetic and copies ran while one was open for 3% of the time, Pallas kernels for 5%

profile of v1, /device:TPU:4, one launch (start us, length us, event | category | flops | bytes accessed | tf_op | source)
XLA Modules:
  0.0 107.7 jit_solution(15755763970436073606)
XLA Ops:
  7.2 0.0 copy-start
  7.2 0.0 copy-start.1
  7.2 0.0 copy-start.2
  7.2 1.1 %copy-done.2 = bf16[512,252]{1,0:T(8,128)(2,1)S(1)} copy-done((bf16[512,252]{1,0:T(8,128)(2,1)S(1)}, bf16[512,252]{1,0:T(8,128)(2,1)}, u32[]{:S(2)}) %copy-start.2) | copy-done | bytes 258072
  8.3 0.9 statistics.1
  9.2 12.8 %all-to-all-start = ((f32[8,8,128]{2,1,0:T(8,128)}), f32[8,8,128]{2,1,0:T(8,128)S(1)}, u32[]{:S(2)}, u32[]{:S(2)}) async-start(f32[8,8,128]{2,1,0:T(8,128)} %statistics.1), calls=%async_computation | async-start | bytes 65536 | tf_op jit(solution)/shard_map/all_to_all | solution.py:227
  21.9 0.0 reduce-scatter.2.cloned.1.call-start
  21.9 0.0 copy-done
  21.9 3.1 %fusion.2.act_grad_ref = f32[512,252]{1,0:T(8,128)} fusion(bf16[512,2016]{0,1:T(8,128)(2,1)} %param.13, bf16[252,2016]{0,1:T(8,128)(2,1)S(1)} %copy-done), kind=kOutput, calls=%fused_computation.11 | convolution fusion | flops 520224768 | bytes 3596544 | tf_op jit(solution)/shard_map/dot_general | solution.py:224
  25.1 0.0 copy-done.8
  25.1 0.0 all-to-all-done.shared_ref
  25.1 2.5 %weight_grad.1 = f32[8,252,252]{2,1,0:T(8,128)} custom-call(f32[8,8,128]{2,1,0:T(8,128)S(1)} %all-to-all-done.shared_ref, bf16[512,252]{1,0:T(8,128)(2,1)S(1)} %copy-done.3, bf16[1,252]{1,0:T(2,128)(2,1)S(1)} %broadcast_in_dim.6.gain_ref, bf16[2016,512]{1,0:T(8,128)(2,1)S(1)} %bitcast.19), custom_call_target="tpu_custom_call" | custom-call | flops 520224768 | bytes 4096512 | tf_op jit(solution)/shard_map/weight_grad/pallas_call | solution.py:115
  27.6 0.0 reduce-scatter.2.cloned.1.call-update
  27.7 1.0 copy-done.4
  28.7 1.4 %norm_grad.1 = (f32[512,252]{1,0:T(8,128)S(1)}, f32[8,8,128]{2,1,0:T(8,128)}) custom-call(f32[8,8,128]{2,1,0:T(8,128)S(1)} %all-to-all-done.shared_ref, bf16[512,252]{1,0:T(8,128)(2,1)S(1)} %copy-done.3, bf16[1,252]{1,0:T(2,128)(2,1)S(1)} %broadcast_in_dim.6.gain_ref, f32[512,252]{1,0:T(8,128)S(1)} %copy-done.4), custom_call_target="tpu_custom_call" | custom-call | flops 2580480 | bytes 1290240 | tf_op jit(solution)/shard_map/norm_grad/pallas_call | solution.py:87
  30.0 5.6 %all-to-all-start.1 = ((f32[8,8,128]{2,1,0:T(8,128)}), f32[8,8,128]{2,1,0:T(8,128)S(1)}, u32[]{:S(2)}, u32[]{:S(2)}) async-start(f32[8,8,128]{2,1,0:T(8,128)} %get-tuple-element.17), calls=%async_computation.1 | async-start | bytes 65536 | tf_op jit(solution)/shard_map/all_to_all | solution.py:227
  35.6 3.0 %all-to-all-done.1 = f32[8,8,128]{2,1,0:T(8,128)S(1)} async-done(((f32[8,8,128]{2,1,0:T(8,128)}), f32[8,8,128]{2,1,0:T(8,128)S(1)}, u32[]{:S(2)}, u32[]{:S(2)}) %all-to-all-start.1) | async-done | bytes 32800 | tf_op jit(solution)/shard_map/all_to_all | solution.py:227
  38.6 0.3 subtract_multiply_fusion.conv_grad_ref
  39.0 1.3 %collective-permute-start = (f32[30,252]{1,0:T(8,128)S(1)}, f32[30,252]{1,0:T(8,128)S(1)}, u32[]{:S(2)}, u32[]{:S(2)}) collective-permute-start(f32[30,252]{1,0:T(8,128)S(1)} %slice.36), channel_id=1, source_target_pairs={{8,0},{16,8},{24,16},{32,24},{40,32},{48,40},{56,48},{64,56},{72,6... | collective-permute-start | bytes 90728 | tf_op jit(solution)/shard_map/ppermute | solution.py:37
  40.3 0.0 copy-done.5
  40.3 0.0 copy-done.6
  40.3 0.0 copy-done.7
  40.3 2.9 %main_rows.1 = (bf16[512,252]{1,0:T(8,128)(2,1)S(1)}, bf16[512,252]{1,0:T(8,128)(2,1)S(1)}, f32[31,8,252]{2,1,0:T(8,128)S(1)}) custom-call(f32[512,252]{1,0:T(8,128)S(1)} %subtract_multiply_fusion.conv_grad_ref, bf16[512,252]{1,0:T(8,128)(2,1)S(1)} %copy-done.5, bf16[512,252]{1,0:T(8,128)(2,1)S(1)} %copy-done.6, bf16[31,252]{1,0:T(8,128)(2,1)S(1)} %copy-done.7), custom_call_target="tpu_custom_call" | custom-call | flops 15998976 | bytes 1548288 | tf_op jit(solution)/shard_map/main_rows/pallas_call | solution.py:195
  43.2 1.6 %collective-permute-done.ahead_ref = f32[30,252]{1,0:T(8,128)S(1)} collective-permute-done((f32[30,252]{1,0:T(8,128)S(1)}, f32[30,252]{1,0:T(8,128)S(1)}, u32[]{:S(2)}, u32[]{:S(2)}) %collective-permute-start) | collective-permute-done | bytes 30272 | tf_op jit(solution)/shard_map/ppermute | solution.py:37
  44.8 1.0 last_rows.1
  45.9 20.4 %all_to_all.25 = f32[12,3,252]{2,1,0:T(4,128)S(1)} all-to-all(f32[12,3,252]{2,1,0:T(4,128)S(1)} %reshape.61), channel_id=1, replica_groups=mesh['z'=12,'y'=8,'tp'=8] {'z'}, dimensions={0} | all-to-all | bytes 72576 | tf_op jit(solution)/shard_map/all_to_all | solution.py:31
  66.3 13.4 %all_to_all.26 = f32[8,3,252]{2,1,0:T(4,128)S(1)} all-to-all(f32[8,3,252]{2,1,0:T(4,128)S(1)} %broadcast_in_dim.7), channel_id=1, replica_groups=mesh['z'=12,'y'=8,'tp'=8] {'y'}, dimensions={0} | all-to-all | bytes 48384 | tf_op jit(solution)/shard_map/all_to_all | solution.py:19
  79.6 0.0 reduce-scatter.2.cloned.1.call-done
  79.7 1.0 reshape_reduce_scatter.3
  80.7 18.8 %all_to_all.27 = f32[12,24,252]{2,1,0:T(8,128)S(1)} all-to-all(f32[12,24,252]{2,1,0:T(8,128)S(1)} %pad_maximum_fusion), channel_id=1, replica_groups=mesh['z'=12,'y'=8,'tp'=8] {'z'}, dimensions={0} | all-to-all | bytes 580608 | tf_op jit(solution)/shard_map/all_to_all | solution.py:251
  99.6 0.6 slice_multiply_fusion
  100.2 0.6 multiply_bitcast_fusion
  (24 shorter events, 0.2 us)
Async XLA Ops:
  7.2 14.8 %copy-start = (bf16[252,2016]{0,1:T(8,128)(2,1)S(1)}, bf16[252,2016]{0,1:T(8,128)(2,1)}, u32[]{:S(2)}) copy-start(bf16[252,2016]{0,1:T(8,128)(2,1)} %param.12) | copy-start | bytes 3048196
  7.2 17.9 %copy-start.1 = (bf16[512,2016]{0,1:T(8,128)(2,1)S(1)}, bf16[512,2016]{0,1:T(8,128)(2,1)}, u32[]{:S(2)}) copy-start(bf16[512,2016]{0,1:T(8,128)(2,1)} %param.13) | copy-start | bytes 6193156
  7.2 1.1 %copy-start.2 = (bf16[512,252]{1,0:T(8,128)(2,1)S(1)}, bf16[512,252]{1,0:T(8,128)(2,1)}, u32[]{:S(2)}) copy-start(bf16[512,252]{1,0:T(8,128)(2,1)} %conv_ref.5) | copy-start | bytes 774148
  8.3 16.8 %copy-start.8 = (bf16[252]{0:T(256)(128)(2,1)S(1)}, bf16[252]{0:T(256)(128)(2,1)}, u32[]{:S(2)}) copy-start(bf16[252]{0:T(256)(128)(2,1)} %param.11) | copy-start | bytes 1516
  8.3 16.8 %copy-start.3 = (bf16[512,252]{1,0:T(8,128)(2,1)S(1)}, bf16[512,252]{1,0:T(8,128)(2,1)}, u32[]{:S(2)}) copy-start(bf16[512,252]{1,0:T(8,128)(2,1)} %conv_ref.5) | copy-start | bytes 774148
  9.2 15.9 %all-to-all-start = ((f32[8,8,128]{2,1,0:T(8,128)}), f32[8,8,128]{2,1,0:T(8,128)S(1)}, u32[]{:S(2)}, u32[]{:S(2)}) async-start(f32[8,8,128]{2,1,0:T(8,128)} %statistics.1), calls=%async_computation | async-start | bytes 65536 | tf_op jit(solution)/shard_map/all_to_all | solution.py:227
  21.9 57.8 %reduce-scatter.2.cloned.1.call-start = ((), (), s32[]{:S(2)}) async-start(), calls=%async_computation.6 | async-start | bytes 2359296 | tf_op jit(solution)/shard_map/reduce_scatter | solution.py:231
  27.6 1.0 copy-start.4
  27.6 12.7 %copy-start.5 = (bf16[512,252]{1,0:T(8,128)(2,1)S(1)}, bf16[512,252]{1,0:T(8,128)(2,1)}, u32[]{:S(2)}) copy-start(bf16[512,252]{1,0:T(8,128)(2,1)} %value_ref.3) | copy-start | bytes 774148
  27.6 12.7 %copy-start.6 = (bf16[512,252]{1,0:T(8,128)(2,1)S(1)}, bf16[512,252]{1,0:T(8,128)(2,1)}, u32[]{:S(2)}) copy-start(bf16[512,252]{1,0:T(8,128)(2,1)} %gate_ref.3) | copy-start | bytes 774148
  27.6 12.7 %copy-start.7 = (bf16[31,252]{1,0:T(8,128)(2,1)S(1)}, bf16[31,252]{1,0:T(8,128)(2,1)}, u32[]{:S(2)}) copy-start(bf16[31,252]{1,0:T(8,128)(2,1)} %taps_ref.3) | copy-start | bytes 46876
  30.0 8.6 %all-to-all-start.1 = ((f32[8,8,128]{2,1,0:T(8,128)}), f32[8,8,128]{2,1,0:T(8,128)S(1)}, u32[]{:S(2)}, u32[]{:S(2)}) async-start(f32[8,8,128]{2,1,0:T(8,128)} %get-tuple-element.17), calls=%async_computation.1 | async-start | bytes 65536 | tf_op jit(solution)/shard_map/all_to_all | solution.py:227
  39.0 5.8 %collective-permute-start = (f32[30,252]{1,0:T(8,128)S(1)}, f32[30,252]{1,0:T(8,128)S(1)}, u32[]{:S(2)}, u32[]{:S(2)}) collective-permute-start(f32[30,252]{1,0:T(8,128)S(1)} %slice.36), channel_id=1, source_target_pairs={{8,0},{16,8},{24,16},{32,24},{40,32},{48,40},{56,48},{64,56},{72,6... | collective-permute-start | bytes 90728 | tf_op jit(solution)/shard_map/ppermute | solution.py:37
Sparse Core Ops, SparseCore 0:
  27.8 46.5 reduce-scatter.1

commit v2 on v1

--- a/solution.py
+++ b/solution.py
@@ -49,9 +49,21 @@
         out_ref[i] = rows
 
 
-def statistics_kernel(conv_ref, out_ref):
-    conv = conv_ref[...].astype(jnp.float32)
-    spread_rows(jnp.sum(conv, axis=1, keepdims=True), jnp.sum(conv * conv, axis=1, keepdims=True), out_ref)
+def statistics_kernel(conv_ref, out_ref, held_ref, sems):
+    parts = sems.shape[0]
+    rows = held_ref.shape[0] // parts
+    copies = []
+    for i in range(parts):
+        part = pl.ds(i * rows, rows)
+        copies.append(pltpu.make_async_copy(conv_ref.at[part], held_ref.at[part], sems.at[i]))
+        copies[i].start()
+    sums, squares = [], []
+    for i in range(parts):
+        copies[i].wait()
+        conv = held_ref[i * rows : (i + 1) * rows].astype(jnp.float32)
+        sums.append(jnp.sum(conv, axis=1, keepdims=True))
+        squares.append(jnp.sum(conv * conv, axis=1, keepdims=True))
+    spread_rows(jnp.concatenate(sums, axis=0), jnp.concatenate(squares, axis=0), out_ref)
 
 
 def statistics(conv_saved, devices):
@@ -59,7 +71,9 @@
         statistics_kernel,
         out_shape=jax.ShapeDtypeStruct((devices, conv_saved.shape[0] // 64, 128), jnp.float32),
         cost_estimate=pl.CostEstimate(flops=3 * conv_saved.size, bytes_accessed=2 * conv_saved.size, transcendentals=0),
-        compiler_params=pltpu.CompilerParams(vmem_limit_bytes=8 * 2**20),
+        in_specs=[pl.BlockSpec(memory_space=pltpu.HBM)],
+        scratch_shapes=[pltpu.VMEM(conv_saved.shape, conv_saved.dtype), pltpu.SemaphoreType.DMA((4,))],
+        compiler_params=pltpu.CompilerParams(vmem_limit_bytes=58 * 2**20),
         name="statistics",
     )(conv_saved)
 
@@ -95,19 +109,29 @@
     )(shared, conv_saved, gain, act_grad)
 
 
-def weight_grad_kernel(model_width, z_size, shared_ref, conv_ref, gain_ref, cot_ref, out_ref, act_ref):
+def weight_grad_kernel(model_width, z_size, shared_ref, conv_ref, gain_ref, cot_ref, out_ref, act_ref, held_ref, sems):
     centered = standardized(model_width, shared_ref, conv_ref)
     normed = centered * gain_ref[...].astype(jnp.float32)
     act_ref[...] = (normed * jax.nn.sigmoid(normed)).astype(jnp.bfloat16)
     y_size = out_ref.shape[0]
     each = out_ref.shape[1] // z_size
     block = 2 * y_size * each
+    early = z_size * 2 // 3 * each
+    copies = [
+        pltpu.make_async_copy(held_ref.at[:, part], out_ref.at[:, part], sems.at[j])
+        for j, part in enumerate((pl.ds(0, early), pl.ds(early, z_size * each - early)))
+    ]
     for i in range(z_size // 2):
+        if 2 * i * each == early:
+            copies[0].start()
         res = jnp.dot(cot_ref[i * block : (i + 1) * block], act_ref[...], preferred_element_type=jnp.float32)
         for g in range(2):
             for y in range(y_size):
                 at, to = (g * y_size + y) * each, (2 * i + g) * each
-                out_ref[y, to : to + each] = res[at : at + each]
+                held_ref[y, to : to + each] = res[at : at + each]
+    copies[1].start()
+    copies[0].wait()
+    copies[1].wait()
 
 
 def weight_grad(shared, conv_saved, gain, cot_t, z_size, y_size):
@@ -115,13 +139,18 @@
     return pl.pallas_call(
         functools.partial(weight_grad_kernel, model_width, z_size),
         out_shape=jax.ShapeDtypeStruct((y_size, model_width // y_size, width), jnp.float32),
-        scratch_shapes=[pltpu.VMEM(conv_saved.shape, jnp.bfloat16)],
+        out_specs=pl.BlockSpec(memory_space=pltpu.HBM),
+        scratch_shapes=[
+            pltpu.VMEM(conv_saved.shape, jnp.bfloat16),
+            pltpu.VMEM((y_size, model_width // y_size, width), jnp.float32),
+            pltpu.SemaphoreType.DMA((2,)),
+        ],
         cost_estimate=pl.CostEstimate(
             flops=2 * conv_saved.size * model_width,
             bytes_accessed=2 * cot_t.size + 4 * model_width * width,
             transcendentals=conv_saved.size,
         ),
-        compiler_params=pltpu.CompilerParams(vmem_limit_bytes=16 * 2**20),
+        compiler_params=pltpu.CompilerParams(vmem_limit_bytes=10 * 2**20),
         name="weight_grad",
     )(shared, conv_saved, gain, cot_t)
 
@@ -212,6 +241,31 @@
         compiler_params=pltpu.CompilerParams(vmem_limit_bytes=12 * 2**20),
         name="last_rows",
     )(conv_grad, ahead, value, gate, taps, *done)
+
+
+def closing_kernel(scale, arrived_ref, weight_out, tap_out):
+    each = weight_out.shape[0]
+    total = arrived_ref[0]
+    for z in range(1, arrived_ref.shape[0]):
+        total = total + arrived_ref[z]
+    weight_out[...] = total[:each] * scale
+    rows = arrived_ref.shape[1] - each
+    for z in range(arrived_ref.shape[0]):
+        at = z * rows
+        count = min(rows, tap_out.shape[0] - at)
+        if count > 0:
+            tap_out[at : at + count] = arrived_ref[z, each : each + count] * scale
+
+
+def closing(arrived, scale, each, tap_count):
+    width = arrived.shape[2]
+    return pl.pallas_call(
+        functools.partial(closing_kernel, scale),
+        out_shape=(jax.ShapeDtypeStruct((each, width), jnp.float32), jax.ShapeDtypeStruct((tap_count, width), jnp.float32)),
+        cost_estimate=pl.CostEstimate(flops=arrived.size, bytes_accessed=4 * arrived.size, transcendentals=0),
+        compiler_params=pltpu.CompilerParams(vmem_limit_bytes=4 * 2**20),
+        name="closing",
+    )(arrived)
 
 
 def local(proj_value, proj_gate, conv_saved, conv_taps, norm_gain, out_weight, cotangent):
@@ -249,8 +303,8 @@
     each = terms.shape[1]
     spread = jnp.broadcast_to(tap_part[None], (z_size, *tap_part.shape))
     arrived = lax.all_to_all(jnp.concatenate([terms, spread], axis=1), "z", 0, 0, tiled=True)
-    grad_out_weight = arrived[:, :each].sum(axis=0).T * grad_scale
-    grad_taps = arrived[:, each:].reshape(-1, arrived.shape[2])[:tap_count] * grad_scale
+    weight_rows, grad_taps = closing(arrived, grad_scale, each, tap_count)
+    grad_out_weight = weight_rows.T
     return (grad_value, grad_gate, grad_out_weight, grad_taps)
 
 

time: 108 us -> 108 us (level)
  Pallas kernels: 8.73 us -> 10.6 us
  other arithmetic: 1.72 us -> 0.46 us
  local copies, waits for them, and re-layouts: 3.18 us -> 2.03 us
    pallas_call x1, Pallas kernels: 0.86 us -> 2.24 us  [statistics(): pl.pallas_call(statistics_kernel, out_shape=jax.ShapeDtypeStruct((devices...]
    mul x2 -> x0, other arithmetic: 1.23 us -> none  [the longest x1 0.62 us: local(): arrived[:, each:].reshape(-1, arrived.shape[2])[:tap_count] * grad_scale]
    unnamed x18 -> x16, local copies, waits for them, and re-layouts: 2.12 us -> 1 us
where the time goes in v2:
time: 108 us; the launch traced here: 107 us
  blocking collectives  52.6 us (49%)
  starting transfers between devices  19.6 us (18%)
  between operations  14.2 us (13%)
  Pallas kernels  10.6 us (10%)
  waiting for transfers between devices  4.6 us (4%)
  matrix products  3.13 us (3%)
  local copies, waits for them, and re-layouts  2.03 us (2%)
    all_to_all x1, blocking collectives, scattered_sum(): return lax.all_to_all(padded, axes, 0, 0, tiled=True).sum(axis=0)  20.4 us
    all_to_all x1, blocking collectives, local(): lax.all_to_all(jnp.concatenate([terms, spread], axis=1), 'z', 0, 0, tiled...  18.9 us
    all_to_all x2, starting transfers between devices, local(): everyone = lambda x: lax.all_to_all(x, 'tp', 0, 0, tiled=True)  18.3 us
    all_to_all x1, blocking collectives, from_everyone(): lax.all_to_all(jnp.broadcast_to(x[None], (size, *x.shape)), axis, 0, 0, t...  13.4 us
    dot_general x1, matrix products, local(): lax.dot_general(cotangent, out_weight, (((1,), (1,)), ((), ())), preferre...  3.13 us
    all_to_all x2, waiting for transfers between devices, local(): everyone = lambda x: lax.all_to_all(x, 'tp', 0, 0, tiled=True)  3.01 us
    pallas_call x1, Pallas kernels, main_rows(): pl.pallas_call(main_rows_kernel, out_shape=(grad, grad, jax.ShapeDtypeStr...  2.91 us
    pallas_call x1, Pallas kernels, weight_grad(): pl.pallas_call(functools.partial(weight_grad_kernel, model_width, z_size)...  2.39 us
  transfers between devices with their start and end apart: 4, of which 2 were waited for; matrix products, arithmetic and copies ran while one was open for 3% of the time, Pallas kernels for 5%

profile of v2, /device:TPU:4, one launch (start us, length us, event | category | flops | bytes accessed | tf_op | source)
XLA Modules:
  0.0 107.3 jit_solution(7695774963837301665)
XLA Ops:
  7.2 0.0 copy-start
  7.2 0.0 copy-start.2
  7.2 0.0 copy-start.1
  7.2 0.0 copy-start.7
  7.2 2.2 %statistics.1 = f32[8,8,128]{2,1,0:T(8,128)} custom-call(bf16[512,252]{1,0:T(8,128)(2,1)} %conv_ref.5), custom_call_target="tpu_custom_call" | custom-call | flops 387072 | bytes 258048 | tf_op jit(solution)/shard_map/statistics/pallas_call | solution.py:70
  9.5 12.8 %all-to-all-start = ((f32[8,8,128]{2,1,0:T(8,128)}), f32[8,8,128]{2,1,0:T(8,128)S(1)}, u32[]{:S(2)}, u32[]{:S(2)}) async-start(f32[8,8,128]{2,1,0:T(8,128)} %statistics.1), calls=%async_computation | async-start | bytes 65536 | tf_op jit(solution)/shard_map/all_to_all | solution.py:281
  22.2 0.0 reduce-scatter.2.cloned.1.call-start
  22.2 0.0 copy-done
  22.2 3.1 %fusion.2.act_grad_ref = f32[512,252]{1,0:T(8,128)} fusion(bf16[512,2016]{0,1:T(8,128)(2,1)} %param.13, bf16[252,2016]{0,1:T(8,128)(2,1)S(1)} %copy-done), kind=kOutput, calls=%fused_computation.8 | convolution fusion | flops 520224768 | bytes 3596544 | tf_op jit(solution)/shard_map/dot_general | solution.py:278
  25.4 0.0 copy-done.7
  25.4 0.0 all-to-all-done.shared_ref
  25.4 2.4 %weight_grad.1 = f32[8,252,252]{2,1,0:T(8,128)} custom-call(f32[8,8,128]{2,1,0:T(8,128)S(1)} %all-to-all-done.shared_ref, bf16[512,252]{1,0:T(8,128)(2,1)S(1)} %copy-done.2, bf16[1,252]{1,0:T(2,128)(2,1)S(1)} %broadcast_in_dim.6.gain_ref, bf16[2016,512]{1,0:T(8,128)(2,1)S(1)} %bitcast.18), custom_call_target="tpu_custom_call" | custom-call | flops 520224768 | bytes 4096512 | tf_op jit(solution)/shard_map/weight_grad/pallas_call | solution.py:139
  27.8 0.0 copy-start.3
  27.8 0.0 copy-start.4
  27.8 0.0 copy-start.5
  27.8 0.0 copy-start.6
  27.8 0.0 reduce-scatter.2.cloned.1.call-update
  27.9 1.0 copy-done.3
  28.8 1.4 %norm_grad.1 = (f32[512,252]{1,0:T(8,128)S(1)}, f32[8,8,128]{2,1,0:T(8,128)}) custom-call(f32[8,8,128]{2,1,0:T(8,128)S(1)} %all-to-all-done.shared_ref, bf16[512,252]{1,0:T(8,128)(2,1)S(1)} %copy-done.2, bf16[1,252]{1,0:T(2,128)(2,1)S(1)} %broadcast_in_dim.6.gain_ref, f32[512,252]{1,0:T(8,128)S(1)} %copy-done.3), custom_call_target="tpu_custom_call" | custom-call | flops 2580480 | bytes 1290240 | tf_op jit(solution)/shard_map/norm_grad/pallas_call | solution.py:101
  30.2 5.5 %all-to-all-start.1 = ((f32[8,8,128]{2,1,0:T(8,128)}), f32[8,8,128]{2,1,0:T(8,128)S(1)}, u32[]{:S(2)}, u32[]{:S(2)}) async-start(f32[8,8,128]{2,1,0:T(8,128)} %get-tuple-element.19), calls=%async_computation.1 | async-start | bytes 65536 | tf_op jit(solution)/shard_map/all_to_all | solution.py:281
  35.8 3.0 %all-to-all-done.1 = f32[8,8,128]{2,1,0:T(8,128)S(1)} async-done(((f32[8,8,128]{2,1,0:T(8,128)}), f32[8,8,128]{2,1,0:T(8,128)S(1)}, u32[]{:S(2)}, u32[]{:S(2)}) %all-to-all-start.1) | async-done | bytes 32800 | tf_op jit(solution)/shard_map/all_to_all | solution.py:281
  38.8 0.3 subtract_multiply_fusion.conv_grad_ref
  39.2 1.3 %collective-permute-start = (f32[30,252]{1,0:T(8,128)S(1)}, f32[30,252]{1,0:T(8,128)S(1)}, u32[]{:S(2)}, u32[]{:S(2)}) collective-permute-start(f32[30,252]{1,0:T(8,128)S(1)} %slice.24), channel_id=1, source_target_pairs={{8,0},{16,8},{24,16},{32,24},{40,32},{48,40},{56,48},{64,56},{72,6... | collective-permute-start | bytes 90728 | tf_op jit(solution)/shard_map/ppermute | solution.py:37
  40.5 2.9 %main_rows.1 = (bf16[512,252]{1,0:T(8,128)(2,1)S(1)}, bf16[512,252]{1,0:T(8,128)(2,1)S(1)}, f32[31,8,252]{2,1,0:T(8,128)S(1)}) custom-call(f32[512,252]{1,0:T(8,128)S(1)} %subtract_multiply_fusion.conv_grad_ref, bf16[512,252]{1,0:T(8,128)(2,1)S(1)} %copy-done.4, bf16[512,252]{1,0:T(8,128)(2,1)S(1)} %copy-done.5, bf16[31,252]{1,0:T(8,128)(2,1)S(1)} %copy-done.6), custom_call_target="tpu_custom_call" | custom-call | flops 15998976 | bytes 1548288 | tf_op jit(solution)/shard_map/main_rows/pallas_call | solution.py:224
  43.4 1.6 %collective-permute-done.ahead_ref = f32[30,252]{1,0:T(8,128)S(1)} collective-permute-done((f32[30,252]{1,0:T(8,128)S(1)}, f32[30,252]{1,0:T(8,128)S(1)}, u32[]{:S(2)}, u32[]{:S(2)}) %collective-permute-start) | collective-permute-done | bytes 30272 | tf_op jit(solution)/shard_map/ppermute | solution.py:37
  45.0 1.0 last_rows.1
  46.0 20.4 %all_to_all.25 = f32[12,3,252]{2,1,0:T(4,128)S(1)} all-to-all(f32[12,3,252]{2,1,0:T(4,128)S(1)} %reshape.58), channel_id=1, replica_groups=mesh['z'=12,'y'=8,'tp'=8] {'z'}, dimensions={0} | all-to-all | bytes 72576 | tf_op jit(solution)/shard_map/all_to_all | solution.py:31
  66.5 13.4 %all_to_all.26 = f32[8,3,252]{2,1,0:T(4,128)S(1)} all-to-all(f32[8,3,252]{2,1,0:T(4,128)S(1)} %broadcast_in_dim.7), channel_id=1, replica_groups=mesh['z'=12,'y'=8,'tp'=8] {'y'}, dimensions={0} | all-to-all | bytes 48384 | tf_op jit(solution)/shard_map/all_to_all | solution.py:19
  79.8 0.0 reduce-scatter.2.cloned.1.call-done
  79.9 1.0 reshape_reduce_scatter.3
  80.9 18.9 %all_to_all.27.arrived_ref = f32[12,24,252]{2,1,0:T(8,128)S(1)} all-to-all(f32[12,24,252]{2,1,0:T(8,128)S(1)} %pad_maximum_fusion), channel_id=1, replica_groups=mesh['z'=12,'y'=8,'tp'=8] {'z'}, dimensions={0} | all-to-all | bytes 580608 | tf_op jit(solution)/shard_map/all_to_all | solution.py:305
  99.8 0.7 closing.1
  (18 shorter events, 0.2 us)
Async XLA Ops:
  7.2 15.1 %copy-start = (bf16[252,2016]{0,1:T(8,128)(2,1)S(1)}, bf16[252,2016]{0,1:T(8,128)(2,1)}, u32[]{:S(2)}) copy-start(bf16[252,2016]{0,1:T(8,128)(2,1)} %param.12) | copy-start | bytes 3048196
  7.2 18.2 %copy-start.2 = (bf16[512,252]{1,0:T(8,128)(2,1)S(1)}, bf16[512,252]{1,0:T(8,128)(2,1)}, u32[]{:S(2)}) copy-start(bf16[512,252]{1,0:T(8,128)(2,1)} %conv_ref.5) | copy-start | bytes 774148
  7.2 18.2 %copy-start.1 = (bf16[512,2016]{0,1:T(8,128)(2,1)S(1)}, bf16[512,2016]{0,1:T(8,128)(2,1)}, u32[]{:S(2)}) copy-start(bf16[512,2016]{0,1:T(8,128)(2,1)} %param.13) | copy-start | bytes 6193156
  7.2 18.2 %copy-start.7 = (bf16[252]{0:T(256)(128)(2,1)S(1)}, bf16[252]{0:T(256)(128)(2,1)}, u32[]{:S(2)}) copy-start(bf16[252]{0:T(256)(128)(2,1)} %param.11) | copy-start | bytes 1516
  9.5 15.9 %all-to-all-start = ((f32[8,8,128]{2,1,0:T(8,128)}), f32[8,8,128]{2,1,0:T(8,128)S(1)}, u32[]{:S(2)}, u32[]{:S(2)}) async-start(f32[8,8,128]{2,1,0:T(8,128)} %statistics.1), calls=%async_computation | async-start | bytes 65536 | tf_op jit(solution)/shard_map/all_to_all | solution.py:281
  22.2 57.6 %reduce-scatter.2.cloned.1.call-start = ((), (), s32[]{:S(2)}) async-start(), calls=%async_computation.6 | async-start | bytes 2359296 | tf_op jit(solution)/shard_map/reduce_scatter | solution.py:285
  27.8 1.0 copy-start.3
  27.8 12.7 %copy-start.4 = (bf16[512,252]{1,0:T(8,128)(2,1)S(1)}, bf16[512,252]{1,0:T(8,128)(2,1)}, u32[]{:S(2)}) copy-start(bf16[512,252]{1,0:T(8,128)(2,1)} %value_ref.3) | copy-start | bytes 774148
  27.8 12.7 %copy-start.5 = (bf16[512,252]{1,0:T(8,128)(2,1)S(1)}, bf16[512,252]{1,0:T(8,128)(2,1)}, u32[]{:S(2)}) copy-start(bf16[512,252]{1,0:T(8,128)(2,1)} %gate_ref.3) | copy-start | bytes 774148
  27.8 12.7 %copy-start.6 = (bf16[31,252]{1,0:T(8,128)(2,1)S(1)}, bf16[31,252]{1,0:T(8,128)(2,1)}, u32[]{:S(2)}) copy-start(bf16[31,252]{1,0:T(8,128)(2,1)} %taps_ref.3) | copy-start | bytes 46876
  30.2 8.6 %all-to-all-start.1 = ((f32[8,8,128]{2,1,0:T(8,128)}), f32[8,8,128]{2,1,0:T(8,128)S(1)}, u32[]{:S(2)}, u32[]{:S(2)}) async-start(f32[8,8,128]{2,1,0:T(8,128)} %get-tuple-element.19), calls=%async_computation.1 | async-start | bytes 65536 | tf_op jit(solution)/shard_map/all_to_all | solution.py:281
  39.2 5.8 %collective-permute-start = (f32[30,252]{1,0:T(8,128)S(1)}, f32[30,252]{1,0:T(8,128)S(1)}, u32[]{:S(2)}, u32[]{:S(2)}) collective-permute-start(f32[30,252]{1,0:T(8,128)S(1)} %slice.24), channel_id=1, source_target_pairs={{8,0},{16,8},{24,16},{32,24},{40,32},{48,40},{56,48},{64,56},{72,6... | collective-permute-start | bytes 90728 | tf_op jit(solution)/shard_map/ppermute | solution.py:37
Sparse Core Ops, SparseCore 0:
  28.0 46.6 reduce-scatter.1

commit v3 on v1

--- a/solution.py
+++ b/solution.py
@@ -134,84 +134,115 @@
         wide_ref[k] = jnp.broadcast_to(taps_ref[k : k + 1].astype(jnp.float32), wide_ref.shape[1:])
 
 
-def filter_rows(window, value, gate, wide_ref, tap_sums_ref):
-    tap_count = wide_ref.shape[0]
+def shifts(window, first, last):
+    for phase in range(8):
+        starts = [at for at in range(first, last + 1) if at % 8 == phase]
+        turned = window[phase : starts[-1] + STEP]
+        for at in starts:
+            yield at, turned[at - phase : at - phase + STEP].reshape(STEP // 8, 8, -1)
+
+
+def gate_of(value, gate):
     gate_proj = jax.nn.sigmoid(gate.astype(jnp.float32))
-    gated = value.astype(jnp.float32) * gate_proj
-    groups = (STEP // 8, 8, gated.shape[1])
-    gated_groups = gated.reshape(groups)
-    d_glu = jnp.zeros(groups, jnp.float32)
-    for phase in range(8):
-        turned = window[phase : phase + 2 * STEP - 8]
-        for at in range(phase, tap_count, 8):
-            k = tap_count - 1 - at
-            shifted = turned[at - phase : at - phase + STEP].reshape(groups)
-            d_glu += wide_ref[k] * shifted
-            tap_sums_ref[k] += (gated_groups * shifted).sum(axis=0)
-    d_glu = d_glu.reshape(gated.shape)
-    grad_value = d_glu * gate_proj
-    grad_gate = d_glu * gated * (1.0 - gate_proj)
-    return grad_value.astype(jnp.bfloat16), grad_gate.astype(jnp.bfloat16)
-
-
-def main_rows_kernel(conv_grad_ref, value_ref, gate_ref, taps_ref, value_out, gate_out, tap_out, wide_ref):
-    tap_out[...] = jnp.zeros_like(tap_out)
-    widen(taps_ref, wide_ref)
+    return gate_proj, value.astype(jnp.float32) * gate_proj
+
+
+def tap_sums_kernel(tap_count, conv_grad_ref, behind_ref, value_ref, gate_ref, out_ref, gated_ref, sums_ref):
+    sums_ref[...] = jnp.zeros_like(sums_ref)
+    gated_ref[:STEP] = behind_ref[...]
+    skipped = STEP - (tap_count - 1)
 
     def one(i, carry):
         at = pl.multiple_of(i * STEP, STEP)
         rows = pl.ds(at, STEP)
-        value_out[rows], gate_out[rows] = filter_rows(
-            conv_grad_ref[pl.ds(at, 2 * STEP)], value_ref[rows], gate_ref[rows], wide_ref, tap_out
-        )
+        gated_ref[pl.ds(pl.multiple_of(at + STEP, STEP), STEP)] = gate_of(value_ref[rows], gate_ref[rows])[1]
+        conv_grad = conv_grad_ref[rows].reshape(STEP // 8, 8, -1)
+        window = gated_ref[pl.ds(at, 2 * STEP)]
+        for start, shifted in shifts(window, skipped, skipped + tap_count - 1):
+            sums_ref[start - skipped] += (conv_grad * shifted).sum(axis=0)
         return carry
 
-    lax.fori_loop(0, value_ref.shape[0] // STEP - 1, one, 0)
+    lax.fori_loop(0, value_ref.shape[0] // STEP, one, 0)
+    out_ref[:tap_count] = jnp.sum(sums_ref[...], axis=1)
+    out_ref[tap_count:] = jnp.zeros((out_ref.shape[0] - tap_count, out_ref.shape[1]), jnp.float32)
+
+
+def tap_sums(conv_grad, behind, value, gate, tap_count, padded_taps):
+    rows, width = value.shape
+    return pl.pallas_call(
+        functools.partial(tap_sums_kernel, tap_count),
+        out_shape=jax.ShapeDtypeStruct((padded_taps, width), jnp.float32),
+        scratch_shapes=[
+            pltpu.VMEM((rows + STEP, width), jnp.float32),
+            pltpu.VMEM((tap_count, 8, width), jnp.float32),
+        ],
+        cost_estimate=pl.CostEstimate(flops=2 * tap_count * value.size, bytes_accessed=8 * value.size, transcendentals=value.size),
+        compiler_params=pltpu.CompilerParams(vmem_limit_bytes=8 * 2**20),
+        name="tap_sums",
+    )(conv_grad, behind, value, gate)
+
+
+def filter_kernel(conv_grad_ref, ahead_ref, value_ref, gate_ref, taps_ref, value_out, gate_out, wide_ref):
+    tap_count, width = taps_ref.shape
+    for k in range(tap_count):
+        wide_ref[k] = jnp.broadcast_to(taps_ref[k : k + 1].astype(jnp.float32), wide_ref.shape[1:])
+
+    def filter_rows(window, rows):
+        gate_proj, gated = gate_of(value_ref[rows], gate_ref[rows])
+        d_glu = jnp.zeros((STEP // 8, 8, width), jnp.float32)
+        for start, shifted in shifts(window, 0, tap_count - 1):
+            d_glu += wide_ref[tap_count - 1 - start] * shifted
+        d_glu = d_glu.reshape(STEP, width)
+        value_out[rows] = (d_glu * gate_proj).astype(jnp.bfloat16)
+        gate_out[rows] = (d_glu * gated * (1.0 - gate_proj)).astype(jnp.bfloat16)
+
+    def one(i, carry):
+        at = pl.multiple_of(i * STEP, STEP)
+        filter_rows(conv_grad_ref[pl.ds(at, 2 * STEP)], pl.ds(at, STEP))
+        return carry
+
     last = value_ref.shape[0] - STEP
-    value_out[last:] = jnp.zeros((STEP, value_out.shape[1]), value_out.dtype)
-    gate_out[last:] = jnp.zeros((STEP, gate_out.shape[1]), gate_out.dtype)
-
-
-def last_rows_kernel(
-    conv_grad_ref, ahead_ref, value_ref, gate_ref, taps_ref, value_in, gate_in, tap_in, value_out, gate_out, tap_out, sums_ref, wide_ref
-):
-    last = value_ref.shape[0] - STEP
-    width = conv_grad_ref.shape[1]
+    lax.fori_loop(0, last // STEP, one, 0)
     ahead = ahead_ref[...]
     fill = jnp.zeros((STEP - ahead.shape[0], width), jnp.float32)
-    window = jnp.concatenate([conv_grad_ref[last:], ahead, fill], axis=0)
-    sums_ref[...] = tap_in[...]
-    widen(taps_ref, wide_ref)
-    value_out[:last] = value_in[:last]
-    gate_out[:last] = gate_in[:last]
-    value_out[last:], gate_out[last:] = filter_rows(window, value_ref[last:], gate_ref[last:], wide_ref, sums_ref)
-    tap_count = taps_ref.shape[0]
-    tap_out[:tap_count] = jnp.sum(sums_ref[...], axis=1)
-    tap_out[tap_count:] = jnp.zeros((tap_out.shape[0] - tap_count, width), jnp.float32)
-
-
-def main_rows(conv_grad, value, gate, taps):
+    filter_rows(jnp.concatenate([conv_grad_ref[last:], ahead, fill], axis=0), pl.ds(last, STEP))
+
+
+def filtered(conv_grad, ahead, value, gate, taps):
     grad = jax.ShapeDtypeStruct(value.shape, jnp.bfloat16)
     return pl.pallas_call(
-        main_rows_kernel,
-        out_shape=(grad, grad, jax.ShapeDtypeStruct((taps.shape[0], 8, taps.shape[1]), jnp.float32)),
+        filter_kernel,
+        out_shape=(grad, grad),
         scratch_shapes=[pltpu.VMEM((taps.shape[0], 8, taps.shape[1]), jnp.float32)],
-        cost_estimate=pl.CostEstimate(flops=4 * taps.shape[0] * value.size, bytes_accessed=12 * value.size, transcendentals=value.size),
-        compiler_params=pltpu.CompilerParams(vmem_limit_bytes=12 * 2**20),
-        name="main_rows",
-    )(conv_grad, value, gate, taps)
-
-
-def last_rows(conv_grad, ahead, value, gate, taps, done, padded_taps):
-    grad = jax.ShapeDtypeStruct(value.shape, jnp.bfloat16)
-    return pl.pallas_call(
-        last_rows_kernel,
-        out_shape=(grad, grad, jax.ShapeDtypeStruct((padded_taps, taps.shape[1]), jnp.float32)),
-        scratch_shapes=[pltpu.VMEM(done[2].shape, jnp.float32)] * 2,
-        cost_estimate=pl.CostEstimate(flops=4 * taps.size * STEP, bytes_accessed=16 * value.size, transcendentals=0),
-        compiler_params=pltpu.CompilerParams(vmem_limit_bytes=12 * 2**20),
-        name="last_rows",
-    )(conv_grad, ahead, value, gate, taps, *done)
+        cost_estimate=pl.CostEstimate(flops=2 * taps.shape[0] * value.size, bytes_accessed=12 * value.size, transcendentals=value.size),
+        compiler_params=pltpu.CompilerParams(vmem_limit_bytes=8 * 2**20),
+        name="filtered",
+    )(conv_grad, ahead, value, gate, taps)
+
+
+def closing_kernel(scale, arrived_ref, weight_out, tap_out):
+    each = weight_out.shape[0]
+    total = arrived_ref[0]
+    for z in range(1, arrived_ref.shape[0]):
+        total = total + arrived_ref[z]
+    weight_out[...] = total[:each] * scale
+    rows = arrived_ref.shape[1] - each
+    for z in range(arrived_ref.shape[0]):
+        at = z * rows
+        count = min(rows, tap_out.shape[0] - at)
+        if count > 0:
+            tap_out[at : at + count] = arrived_ref[z, each : each + count] * scale
+
+
+def closing(arrived, scale, each, tap_count):
+    width = arrived.shape[2]
+    return pl.pallas_call(
+        functools.partial(closing_kernel, scale),
+        out_shape=(jax.ShapeDtypeStruct((each, width), jnp.float32), jax.ShapeDtypeStruct((tap_count, width), jnp.float32)),
+        cost_estimate=pl.CostEstimate(flops=arrived.size, bytes_accessed=4 * arrived.size, transcendentals=0),
+        compiler_params=pltpu.CompilerParams(vmem_limit_bytes=4 * 2**20),
+        name="closing",
+    )(arrived)
 
 
 def local(proj_value, proj_gate, conv_saved, conv_taps, norm_gain, out_weight, cotangent):
@@ -231,7 +262,9 @@
     terms = lax.psum_scatter(terms, "y", scatter_dimension=0)
     terms = terms.reshape(z_size, -1, terms.shape[1])
     d_hat, moments = norm_grad(model_width, shared, conv_saved, norm_gain[None], d_act)
+    moments, value_end, gate_end = lax.optimization_barrier((moments, proj_value[-STEP:], proj_gate[-STEP:]))
     moments = everyone(moments)
+    behind = passed_along(gate_of(value_end, gate_end)[1], SP, 1)
     totals = shared.sum(axis=0).reshape(2, tok_rows)
     row_mean = totals[0] / model_width
     row_var = totals[1] / model_width - row_mean * row_mean
@@ -241,16 +274,17 @@
     first = moments[0] / model_width
     second = moments[1] / model_width
     d_conv = inv_std[:, None] * (d_hat - first[:, None] - centered * second[:, None])
-    ahead = passed_along(d_conv[:overhang], SP, -1)
-    done = main_rows(d_conv, proj_value, proj_gate, conv_taps)
     padded_taps = -(-tap_count // z_size) * z_size
-    grad_value, grad_gate, tap_sums = last_rows(d_conv, ahead, proj_value, proj_gate, conv_taps, done, padded_taps)
-    tap_part = taken_together(scattered_sum(tap_sums, "z"), "y")
+    sums = tap_sums(d_conv, behind, proj_value, proj_gate, tap_count, padded_taps)
+    head, sums = lax.optimization_barrier((d_conv[:overhang], sums))
+    ahead = passed_along(head, SP, -1)
+    grad_value, grad_gate = filtered(d_conv, ahead, proj_value, proj_gate, conv_taps)
+    tap_part = taken_together(scattered_sum(sums, "z"), "y")
     each = terms.shape[1]
     spread = jnp.broadcast_to(tap_part[None], (z_size, *tap_part.shape))
     arrived = lax.all_to_all(jnp.concatenate([terms, spread], axis=1), "z", 0, 0, tiled=True)
-    grad_out_weight = arrived[:, :each].sum(axis=0).T * grad_scale
-    grad_taps = arrived[:, each:].reshape(-1, arrived.shape[2])[:tap_count] * grad_scale
+    weight_rows, grad_taps = closing(arrived, grad_scale, each, tap_count)
+    grad_out_weight = weight_rows.T
     return (grad_value, grad_gate, grad_out_weight, grad_taps)
 
 

time: 108 us -> 109 us (level)
  the two profiles are of different devices: /device:TPU:4 before, /device:TPU:2 now
where the time goes in v3:
time: 109 us; the launch traced here: 108 us
  blocking collectives  35.4 us (32%)
  starting transfers between devices  27.2 us (25%)
  between operations  14.2 us (13%)
  waiting for transfers between devices  13.5 us (12%)
  Pallas kernels  10.2 us (9%)
  local copies, waits for them, and re-layouts  3.15 us (3%)
  matrix products  3.13 us (3%)
  other arithmetic  1.2 us (1%)
    all_to_all x1, blocking collectives, scattered_sum(): return lax.all_to_all(padded, axes, 0, 0, tiled=True).sum(axis=0)  21.4 us
    all_to_all x2, starting transfers between devices, local(): everyone = lambda x: lax.all_to_all(x, 'tp', 0, 0, tiled=True)  17.5 us
    all_to_all x1, blocking collectives, from_everyone(): lax.all_to_all(jnp.broadcast_to(x[None], (size, *x.shape)), axis, 0, 0, t...  14 us
    all_to_all x1, starting transfers between devices, local(): lax.all_to_all(jnp.concatenate([terms, spread], axis=1), 'z', 0, 0, tiled...  7.17 us
    all_to_all x1, waiting for transfers between devices, local(): lax.all_to_all(jnp.concatenate([terms, spread], axis=1), 'z', 0, 0, tiled...  5.41 us
    ppermute x2, waiting for transfers between devices, passed_along(): return lax.ppermute(block, axis, route)  4.51 us
    all_to_all x2, waiting for transfers between devices, local(): everyone = lambda x: lax.all_to_all(x, 'tp', 0, 0, tiled=True)  3.52 us
    dot_general x1, matrix products, local(): lax.dot_general(cotangent, out_weight, (((1,), (1,)), ((), ())), preferre...  3.13 us
  transfers between devices with their start and end apart: 6, of which 4 were waited for; matrix products, arithmetic and copies ran while one was open for 3% of the time, Pallas kernels for 6%

profile of v3, /device:TPU:2, one launch (start us, length us, event | category | flops | bytes accessed | tf_op | source)
XLA Modules:
  0.0 108.0 jit_solution(932248916630990544)
XLA Ops:
  7.2 0.0 copy-start
  7.2 0.0 copy-start.1
  7.2 0.0 copy-start.2
  7.2 1.1 %copy-done.2 = bf16[512,252]{1,0:T(8,128)(2,1)S(1)} copy-done((bf16[512,252]{1,0:T(8,128)(2,1)S(1)}, bf16[512,252]{1,0:T(8,128)(2,1)}, u32[]{:S(2)}) %copy-start.2) | copy-done | bytes 258072
  8.3 0.9 statistics.1
  9.2 12.8 %all-to-all-start = ((f32[8,8,128]{2,1,0:T(8,128)}), f32[8,8,128]{2,1,0:T(8,128)S(1)}, u32[]{:S(2)}, u32[]{:S(2)}) async-start(f32[8,8,128]{2,1,0:T(8,128)} %statistics.1), calls=%async_computation | async-start | bytes 65536 | tf_op jit(solution)/shard_map/all_to_all | solution.py:258
  21.9 0.0 reduce-scatter.2.cloned.1.call-start
  21.9 3.1 %fusion.2.act_grad_ref = f32[512,252]{1,0:T(8,128)} fusion(bf16[512,2016]{0,1:T(8,128)(2,1)} %param.13, bf16[252,2016]{0,1:T(8,128)(2,1)S(1)} %copy-done), kind=kOutput, calls=%fused_computation.9 | convolution fusion | flops 520224768 | bytes 3596544 | tf_op jit(solution)/shard_map/dot_general | solution.py:255
  25.1 0.9 all-to-all-done.shared_ref
  25.9 0.0 copy-done.3
  26.0 2.5 %weight_grad.1 = f32[8,252,252]{2,1,0:T(8,128)} custom-call(f32[8,8,128]{2,1,0:T(8,128)S(1)} %all-to-all-done.shared_ref, bf16[512,252]{1,0:T(8,128)(2,1)S(1)} %copy-done.3, bf16[1,252]{1,0:T(2,128)(2,1)S(1)} %broadcast_in_dim.6.gain_ref, bf16[2016,512]{1,0:T(8,128)(2,1)S(1)} %bitcast.18), custom_call_target="tpu_custom_call" | custom-call | flops 520224768 | bytes 4096512 | tf_op jit(solution)/shard_map/weight_grad/pallas_call | solution.py:115
  28.5 0.0 reduce-scatter.2.cloned.1.call-update
  28.5 1.0 copy-done.4
  29.5 1.4 %norm_grad.1 = (f32[512,252]{1,0:T(8,128)S(1)}, f32[8,8,128]{2,1,0:T(8,128)}) custom-call(f32[8,8,128]{2,1,0:T(8,128)S(1)} %all-to-all-done.shared_ref, bf16[512,252]{1,0:T(8,128)(2,1)S(1)} %copy-done.3, bf16[1,252]{1,0:T(2,128)(2,1)S(1)} %broadcast_in_dim.6.gain_ref, f32[512,252]{1,0:T(8,128)S(1)} %copy-done.4), custom_call_target="tpu_custom_call" | custom-call | flops 2580480 | bytes 1290240 | tf_op jit(solution)/shard_map/norm_grad/pallas_call | solution.py:87
  30.9 4.7 %all-to-all-start.1 = ((f32[8,8,128]{2,1,0:T(8,128)}), f32[8,8,128]{2,1,0:T(8,128)S(1)}, u32[]{:S(2)}, u32[]{:S(2)}) async-start(f32[8,8,128]{2,1,0:T(8,128)} %get-tuple-element.21), calls=%async_computation.1 | async-start | bytes 65536 | tf_op jit(solution)/shard_map/all_to_all | solution.py:258
  35.7 1.3 %collective-permute-start = (f32[32,252]{1,0:T(8,128)S(1)}, f32[32,252]{1,0:T(8,128)S(1)}, u32[]{:S(2)}, u32[]{:S(2)}) collective-permute-start(f32[32,252]{1,0:T(8,128)S(1)} %divide_multiply_fusion), channel_id=1, source_target_pairs={{0,8},{8,16},{16,24},{24,32},{32,40},{40,48},{48,56},{56,64},{64,7... | collective-permute-start | bytes 96776 | tf_op jit(solution)/shard_map/ppermute | solution.py:37
  37.0 2.7 %all-to-all-done.1 = f32[8,8,128]{2,1,0:T(8,128)S(1)} async-done(((f32[8,8,128]{2,1,0:T(8,128)}), f32[8,8,128]{2,1,0:T(8,128)S(1)}, u32[]{:S(2)}, u32[]{:S(2)}) %all-to-all-start.1) | async-done | bytes 32800 | tf_op jit(solution)/shard_map/all_to_all | solution.py:258
  39.6 0.3 subtract_multiply_fusion.conv_grad_ref
  40.0 0.0 collective-permute-done.behind_ref
  40.0 0.0 copy-done.5
  40.0 2.1 %tap_sums.1 = f32[36,252]{1,0:T(8,128)S(1)} custom-call(f32[512,252]{1,0:T(8,128)S(1)} %subtract_multiply_fusion.conv_grad_ref, f32[32,252]{1,0:T(8,128)S(1)} %collective-permute-done.behind_ref, bf16[512,252]{1,0:T(8,128)(2,1)S(1)} %copy-done.5, bf16[512,252]{1,0:T(8,128)(2,1)S(1)} %copy-done.6), custom_call_target="tpu_custom_call" | custom-call | flops 7999488 | bytes 1032192 | tf_op jit(solution)/shard_map/tap_sums/pallas_call | solution.py:172
  42.2 21.4 %all_to_all.25 = f32[12,3,252]{2,1,0:T(4,128)S(1)} all-to-all(f32[12,3,252]{2,1,0:T(4,128)S(1)} %reshape.58), channel_id=1, replica_groups=mesh['z'=12,'y'=8,'tp'=8] {'z'}, dimensions={0} | all-to-all | bytes 72576 | tf_op jit(solution)/shard_map/all_to_all | solution.py:31
  63.7 14.0 %all_to_all.26 = f32[8,3,252]{2,1,0:T(4,128)S(1)} all-to-all(f32[8,3,252]{2,1,0:T(4,128)S(1)} %broadcast_in_dim.7), channel_id=1, replica_groups=mesh['z'=12,'y'=8,'tp'=8] {'y'}, dimensions={0} | all-to-all | bytes 48384 | tf_op jit(solution)/shard_map/all_to_all | solution.py:19
  77.7 0.0 reduce-scatter.2.cloned.1.call-done
  77.7 1.0 reshape_reduce_scatter.3
  78.7 0.8 pad_maximum_fusion
  79.5 7.2 %all-to-all-start.4 = ((f32[12,24,252]{2,1,0:T(8,128)}), f32[12,24,252]{2,1,0:T(8,128)S(1)}, u32[]{:S(2)}, u32[]{:S(2)}) async-start(f32[12,24,252]{2,1,0:T(8,128)} %pad_maximum_fusion), calls=%async_computation.5 | async-start | bytes 589824 | tf_op jit(solution)/shard_map/all_to_all | solution.py:285
  86.7 1.3 %collective-permute-start.1 = (f32[30,252]{1,0:T(8,128)S(1)}, f32[30,252]{1,0:T(8,128)S(1)}, u32[]{:S(2)}, u32[]{:S(2)}) collective-permute-start(f32[30,252]{1,0:T(8,128)S(1)} %slice.32), channel_id=1, source_target_pairs={{8,0},{16,8},{24,16},{32,24},{40,32},{48,40},{56,48},{64,56},{72,6... | collective-permute-start | bytes 90728 | tf_op jit(solution)/shard_map/ppermute | solution.py:37
  88.0 4.5 %collective-permute-done.1.ahead_ref = f32[30,252]{1,0:T(8,128)S(1)} collective-permute-done((f32[30,252]{1,0:T(8,128)S(1)}, f32[30,252]{1,0:T(8,128)S(1)}, u32[]{:S(2)}, u32[]{:S(2)}) %collective-permute-start.1) | collective-permute-done | bytes 30272 | tf_op jit(solution)/shard_map/ppermute | solution.py:37
  92.5 2.7 %filtered.1 = (bf16[512,252]{1,0:T(8,128)(2,1)}, bf16[512,252]{1,0:T(8,128)(2,1)}) custom-call(f32[512,252]{1,0:T(8,128)S(1)} %subtract_multiply_fusion.conv_grad_ref, f32[30,252]{1,0:T(8,128)S(1)} %collective-permute-done.1.ahead_ref, bf16[512,252]{1,0:T(8,128)(2,1)S(1)} %copy-done.5, bf16[512,252]{1,0:T(8,128)(2,1)S(1)} %copy-done.6, ...), custom_call_target="tpu_custom_call" | custom-call | flops 7999488 | bytes 1548288 | tf_op jit(solution)/shard_map/filtered/pallas_call | solution.py:213
  95.1 5.4 %all-to-all-done.4.arrived_ref = f32[12,24,252]{2,1,0:T(8,128)S(1)} async-done(((f32[12,24,252]{2,1,0:T(8,128)}), f32[12,24,252]{2,1,0:T(8,128)S(1)}, u32[]{:S(2)}, u32[]{:S(2)}) %all-to-all-start.4) | async-done | bytes 290336 | tf_op jit(solution)/shard_map/all_to_all | solution.py:285
  100.5 0.7 closing.1
  (28 shorter events, 0.2 us)
Async XLA Ops:
  7.2 14.8 %copy-start = (bf16[252,2016]{0,1:T(8,128)(2,1)S(1)}, bf16[252,2016]{0,1:T(8,128)(2,1)}, u32[]{:S(2)}) copy-start(bf16[252,2016]{0,1:T(8,128)(2,1)} %param.12) | copy-start | bytes 3048196
  7.2 18.8 %copy-start.1 = (bf16[512,2016]{0,1:T(8,128)(2,1)S(1)}, bf16[512,2016]{0,1:T(8,128)(2,1)}, u32[]{:S(2)}) copy-start(bf16[512,2016]{0,1:T(8,128)(2,1)} %param.13) | copy-start | bytes 6193156
  7.2 1.1 %copy-start.2 = (bf16[512,252]{1,0:T(8,128)(2,1)S(1)}, bf16[512,252]{1,0:T(8,128)(2,1)}, u32[]{:S(2)}) copy-start(bf16[512,252]{1,0:T(8,128)(2,1)} %conv_ref.5) | copy-start | bytes 774148
  8.3 16.8 %copy-start.8 = (bf16[252]{0:T(256)(128)(2,1)S(1)}, bf16[252]{0:T(256)(128)(2,1)}, u32[]{:S(2)}) copy-start(bf16[252]{0:T(256)(128)(2,1)} %param.11) | copy-start | bytes 1516
  8.3 17.7 %copy-start.3 = (bf16[512,252]{1,0:T(8,128)(2,1)S(1)}, bf16[512,252]{1,0:T(8,128)(2,1)}, u32[]{:S(2)}) copy-start(bf16[512,252]{1,0:T(8,128)(2,1)} %conv_ref.5) | copy-start | bytes 774148
  9.2 16.8 %all-to-all-start = ((f32[8,8,128]{2,1,0:T(8,128)}), f32[8,8,128]{2,1,0:T(8,128)S(1)}, u32[]{:S(2)}, u32[]{:S(2)}) async-start(f32[8,8,128]{2,1,0:T(8,128)} %statistics.1), calls=%async_computation | async-start | bytes 65536 | tf_op jit(solution)/shard_map/all_to_all | solution.py:258
  21.9 55.8 %reduce-scatter.2.cloned.1.call-start = ((), (), s32[]{:S(2)}) async-start(), calls=%async_computation.6 | async-start | bytes 2359296 | tf_op jit(solution)/shard_map/reduce_scatter | solution.py:262
  28.5 1.0 copy-start.4
  28.5 7.1 %slice-start = ((bf16[512,252]{1,0:T(8,128)(2,1)}), bf16[32,252]{1,0:T(8,128)(2,1)S(1)}, s32[]{:S(2)}) async-start(bf16[512,252]{1,0:T(8,128)(2,1)} %value_ref.3), calls=%async_computation.7 | async-start | bytes 32768 | tf_op jit(solution)/shard_map/slice | solution.py:265
  28.5 7.1 %slice-start.1 = ((bf16[512,252]{1,0:T(8,128)(2,1)}), bf16[32,252]{1,0:T(8,128)(2,1)S(1)}, s32[]{:S(2)}) async-start(bf16[512,252]{1,0:T(8,128)(2,1)} %gate_ref.3), calls=%async_computation.8 | async-start | bytes 32768 | tf_op jit(solution)/shard_map/slice | solution.py:265
  28.5 11.5 %copy-start.5 = (bf16[512,252]{1,0:T(8,128)(2,1)S(1)}, bf16[512,252]{1,0:T(8,128)(2,1)}, u32[]{:S(2)}) copy-start(bf16[512,252]{1,0:T(8,128)(2,1)} %value_ref.3) | copy-start | bytes 774148
  28.5 11.5 %copy-start.6 = (bf16[512,252]{1,0:T(8,128)(2,1)S(1)}, bf16[512,252]{1,0:T(8,128)(2,1)}, u32[]{:S(2)}) copy-start(bf16[512,252]{1,0:T(8,128)(2,1)} %gate_ref.3) | copy-start | bytes 774148
  30.9 8.7 %all-to-all-start.1 = ((f32[8,8,128]{2,1,0:T(8,128)}), f32[8,8,128]{2,1,0:T(8,128)S(1)}, u32[]{:S(2)}, u32[]{:S(2)}) async-start(f32[8,8,128]{2,1,0:T(8,128)} %get-tuple-element.21), calls=%async_computation.1 | async-start | bytes 65536 | tf_op jit(solution)/shard_map/all_to_all | solution.py:258
  35.7 4.3 %collective-permute-start = (f32[32,252]{1,0:T(8,128)S(1)}, f32[32,252]{1,0:T(8,128)S(1)}, u32[]{:S(2)}, u32[]{:S(2)}) collective-permute-start(f32[32,252]{1,0:T(8,128)S(1)} %divide_multiply_fusion), channel_id=1, source_target_pairs={{0,8},{8,16},{16,24},{24,32},{32,40},{40,48},{48,56},{56,64},{64,7... | collective-permute-start | bytes 96776 | tf_op jit(solution)/shard_map/ppermute | solution.py:37
  39.6 52.8 %copy-start.7 = (bf16[31,252]{1,0:T(8,128)(2,1)S(1)}, bf16[31,252]{1,0:T(8,128)(2,1)}, u32[]{:S(2)}) copy-start(bf16[31,252]{1,0:T(8,128)(2,1)} %taps_ref.1) | copy-start | bytes 46876
  79.5 21.1 %all-to-all-start.4 = ((f32[12,24,252]{2,1,0:T(8,128)}), f32[12,24,252]{2,1,0:T(8,128)S(1)}, u32[]{:S(2)}, u32[]{:S(2)}) async-start(f32[12,24,252]{2,1,0:T(8,128)} %pad_maximum_fusion), calls=%async_computation.5 | async-start | bytes 589824 | tf_op jit(solution)/shard_map/all_to_all | solution.py:285
  86.7 5.8 %collective-permute-start.1 = (f32[30,252]{1,0:T(8,128)S(1)}, f32[30,252]{1,0:T(8,128)S(1)}, u32[]{:S(2)}, u32[]{:S(2)}) collective-permute-start(f32[30,252]{1,0:T(8,128)S(1)} %slice.32), channel_id=1, source_target_pairs={{8,0},{16,8},{24,16},{32,24},{40,32},{48,40},{56,48},{64,56},{72,6... | collective-permute-start | bytes 90728 | tf_op jit(solution)/shard_map/ppermute | solution.py:37
Sparse Core Ops, SparseCore 0:
  28.6 45.8 reduce-scatter.1

commit v4 on v3

--- a/solution.py
+++ b/solution.py
@@ -279,7 +279,9 @@
     head, sums = lax.optimization_barrier((d_conv[:overhang], sums))
     ahead = passed_along(head, SP, -1)
     grad_value, grad_gate = filtered(d_conv, ahead, proj_value, proj_gate, conv_taps)
-    tap_part = taken_together(scattered_sum(sums, "z"), "y")
+    tap_part = scattered_sum(sums, "z")
+    tap_part, grad_value, grad_gate = lax.optimization_barrier((tap_part, grad_value, grad_gate))
+    tap_part = taken_together(tap_part, "y")
     each = terms.shape[1]
     spread = jnp.broadcast_to(tap_part[None], (z_size, *tap_part.shape))
     arrived = lax.all_to_all(jnp.concatenate([terms, spread], axis=1), "z", 0, 0, tiled=True)

time: 109 us -> 109 us (level)
  the two profiles are of different devices: /device:TPU:2 before, /device:TPU:4 now
where the time goes in v4:
time: 109 us
  blocking collectives  35.7 us (33%)
  starting transfers between devices  32.7 us (30%)
  between operations  14.2 us (13%)
  Pallas kernels  10.2 us (9%)
  waiting for transfers between devices  8.57 us (8%)
  local copies, waits for them, and re-layouts  3.76 us (3%)
  matrix products  3.13 us (3%)
    all_to_all x1, blocking collectives, local(): lax.all_to_all(jnp.concatenate([terms, spread], axis=1), 'z', 0, 0, tiled...  21.7 us
    all_to_all x2, starting transfers between devices, local(): everyone = lambda x: lax.all_to_all(x, 'tp', 0, 0, tiled=True)  18.3 us
    all_to_all x1, blocking collectives, from_everyone(): lax.all_to_all(jnp.broadcast_to(x[None], (size, *x.shape)), axis, 0, 0, t...  14 us
    all_to_all x1, starting transfers between devices, scattered_sum(): return lax.all_to_all(padded, axes, 0, 0, tiled=True).sum(axis=0)  11.8 us
    ppermute x2, waiting for transfers between devices, passed_along(): return lax.ppermute(block, axis, route)  5.08 us
    dot_general x1, matrix products, local(): lax.dot_general(cotangent, out_weight, (((1,), (1,)), ((), ())), preferre...  3.13 us
    pallas_call x1, Pallas kernels, filtered(): pl.pallas_call(filter_kernel, out_shape=(grad, grad), scratch_shapes=[plt...  2.66 us
    ppermute x2, starting transfers between devices, passed_along(): return lax.ppermute(block, axis, route)  2.58 us
  transfers between devices with their start and end apart: 6, of which 3 were waited for; matrix products, arithmetic and copies ran while one was open for 4% of the time, Pallas kernels for 6%

profile of v4, /device:TPU:4, one launch (start us, length us, event | category | flops | bytes accessed | tf_op | source)
XLA Modules:
  0.0 108.7 jit_solution(9448323059223783429)
XLA Ops:
  7.2 0.0 copy-start
  7.2 0.0 copy-start.1
  7.2 0.0 copy-start.2
  7.2 1.1 %copy-done.2 = bf16[512,252]{1,0:T(8,128)(2,1)S(1)} copy-done((bf16[512,252]{1,0:T(8,128)(2,1)S(1)}, bf16[512,252]{1,0:T(8,128)(2,1)}, u32[]{:S(2)}) %copy-start.2) | copy-done | bytes 258072
  8.3 0.9 statistics.1
  9.2 12.8 %all-to-all-start = ((f32[8,8,128]{2,1,0:T(8,128)}), f32[8,8,128]{2,1,0:T(8,128)S(1)}, u32[]{:S(2)}, u32[]{:S(2)}) async-start(f32[8,8,128]{2,1,0:T(8,128)} %statistics.1), calls=%async_computation | async-start | bytes 65536 | tf_op jit(solution)/shard_map/all_to_all | solution.py:258
  21.9 0.0 reduce-scatter.2.cloned.1.call-start
  21.9 3.1 %fusion.2.act_grad_ref = f32[512,252]{1,0:T(8,128)} fusion(bf16[512,2016]{0,1:T(8,128)(2,1)} %param.13, bf16[252,2016]{0,1:T(8,128)(2,1)S(1)} %copy-done), kind=kOutput, calls=%fused_computation.9 | convolution fusion | flops 520224768 | bytes 3596544 | tf_op jit(solution)/shard_map/dot_general | solution.py:255
  25.1 0.0 copy-done.8
  25.1 0.0 all-to-all-done.shared_ref
  25.1 2.5 %weight_grad.1 = f32[8,252,252]{2,1,0:T(8,128)} custom-call(f32[8,8,128]{2,1,0:T(8,128)S(1)} %all-to-all-done.shared_ref, bf16[512,252]{1,0:T(8,128)(2,1)S(1)} %copy-done.3, bf16[1,252]{1,0:T(2,128)(2,1)S(1)} %broadcast_in_dim.6.gain_ref, bf16[2016,512]{1,0:T(8,128)(2,1)S(1)} %bitcast.18), custom_call_target="tpu_custom_call" | custom-call | flops 520224768 | bytes 4096512 | tf_op jit(solution)/shard_map/weight_grad/pallas_call | solution.py:115
  27.6 0.0 reduce-scatter.2.cloned.1.call-update
  27.7 0.0 copy-start.7
  27.7 1.0 copy-done.4
  28.7 1.4 %norm_grad.1 = (f32[512,252]{1,0:T(8,128)S(1)}, f32[8,8,128]{2,1,0:T(8,128)}) custom-call(f32[8,8,128]{2,1,0:T(8,128)S(1)} %all-to-all-done.shared_ref, bf16[512,252]{1,0:T(8,128)(2,1)S(1)} %copy-done.3, bf16[1,252]{1,0:T(2,128)(2,1)S(1)} %broadcast_in_dim.6.gain_ref, f32[512,252]{1,0:T(8,128)S(1)} %copy-done.4), custom_call_target="tpu_custom_call" | custom-call | flops 2580480 | bytes 1290240 | tf_op jit(solution)/shard_map/norm_grad/pallas_call | solution.py:87
  30.0 5.5 %all-to-all-start.1 = ((f32[8,8,128]{2,1,0:T(8,128)}), f32[8,8,128]{2,1,0:T(8,128)S(1)}, u32[]{:S(2)}, u32[]{:S(2)}) async-start(f32[8,8,128]{2,1,0:T(8,128)} %get-tuple-element.24), calls=%async_computation.1 | async-start | bytes 65536 | tf_op jit(solution)/shard_map/all_to_all | solution.py:258
  35.6 1.3 %collective-permute-start = (f32[32,252]{1,0:T(8,128)S(1)}, f32[32,252]{1,0:T(8,128)S(1)}, u32[]{:S(2)}, u32[]{:S(2)}) collective-permute-start(f32[32,252]{1,0:T(8,128)S(1)} %divide_multiply_fusion), channel_id=1, source_target_pairs={{0,8},{8,16},{16,24},{24,32},{32,40},{40,48},{48,56},{56,64},{64,7... | collective-permute-start | bytes 96776 | tf_op jit(solution)/shard_map/ppermute | solution.py:37
  36.9 1.7 %all-to-all-done.1 = f32[8,8,128]{2,1,0:T(8,128)S(1)} async-done(((f32[8,8,128]{2,1,0:T(8,128)}), f32[8,8,128]{2,1,0:T(8,128)S(1)}, u32[]{:S(2)}, u32[]{:S(2)}) %all-to-all-start.1) | async-done | bytes 32800 | tf_op jit(solution)/shard_map/all_to_all | solution.py:258
  38.6 0.3 subtract_multiply_fusion.conv_grad_ref
  39.0 0.0 collective-permute-done.behind_ref
  39.0 2.1 %tap_sums.1 = f32[36,252]{1,0:T(8,128)S(1)} custom-call(f32[512,252]{1,0:T(8,128)S(1)} %subtract_multiply_fusion.conv_grad_ref, f32[32,252]{1,0:T(8,128)S(1)} %collective-permute-done.behind_ref, bf16[512,252]{1,0:T(8,128)(2,1)S(1)} %copy-done.5, bf16[512,252]{1,0:T(8,128)(2,1)S(1)} %copy-done.6), custom_call_target="tpu_custom_call" | custom-call | flops 7999488 | bytes 1032192 | tf_op jit(solution)/shard_map/tap_sums/pallas_call | solution.py:172
  41.2 0.6 reshape.58
  41.8 11.8 %all-to-all-start.2 = ((f32[12,3,252]{2,1,0:T(4,128)}), f32[12,3,252]{2,1,0:T(4,128)S(1)}, u32[]{:S(2)}, u32[]{:S(2)}) async-start(f32[12,3,252]{2,1,0:T(4,128)} %reshape.58), calls=%async_computation.2 | async-start | bytes 98304 | tf_op jit(solution)/shard_map/all_to_all | solution.py:31
  53.6 1.3 %collective-permute-start.1 = (f32[30,252]{1,0:T(8,128)S(1)}, f32[30,252]{1,0:T(8,128)S(1)}, u32[]{:S(2)}, u32[]{:S(2)}) collective-permute-start(f32[30,252]{1,0:T(8,128)S(1)} %slice.32), channel_id=1, source_target_pairs={{8,0},{16,8},{24,16},{32,24},{40,32},{48,40},{56,48},{64,56},{72,6... | collective-permute-start | bytes 90728 | tf_op jit(solution)/shard_map/ppermute | solution.py:37
  54.9 5.1 %collective-permute-done.1.ahead_ref = f32[30,252]{1,0:T(8,128)S(1)} collective-permute-done((f32[30,252]{1,0:T(8,128)S(1)}, f32[30,252]{1,0:T(8,128)S(1)}, u32[]{:S(2)}, u32[]{:S(2)}) %collective-permute-start.1) | collective-permute-done | bytes 30272 | tf_op jit(solution)/shard_map/ppermute | solution.py:37
  60.0 2.7 %filtered.1 = (bf16[512,252]{1,0:T(8,128)(2,1)}, bf16[512,252]{1,0:T(8,128)(2,1)}) custom-call(f32[512,252]{1,0:T(8,128)S(1)} %subtract_multiply_fusion.conv_grad_ref, f32[30,252]{1,0:T(8,128)S(1)} %collective-permute-done.1.ahead_ref, bf16[512,252]{1,0:T(8,128)(2,1)S(1)} %copy-done.5, bf16[512,252]{1,0:T(8,128)(2,1)S(1)} %copy-done.6, ...), custom_call_target="tpu_custom_call" | custom-call | flops 7999488 | bytes 1548288 | tf_op jit(solution)/shard_map/filtered/pallas_call | solution.py:213
  62.6 1.8 %all-to-all-done.2 = f32[12,3,252]{2,1,0:T(4,128)S(1)} async-done(((f32[12,3,252]{2,1,0:T(4,128)}), f32[12,3,252]{2,1,0:T(4,128)S(1)}, u32[]{:S(2)}, u32[]{:S(2)}) %all-to-all-start.2) | async-done | bytes 36320 | tf_op jit(solution)/shard_map/all_to_all | solution.py:31
  64.5 14.0 %all_to_all.25 = f32[8,3,252]{2,1,0:T(4,128)S(1)} all-to-all(f32[8,3,252]{2,1,0:T(4,128)S(1)} %broadcast_in_dim.7), channel_id=1, replica_groups=mesh['z'=12,'y'=8,'tp'=8] {'y'}, dimensions={0} | all-to-all | bytes 48384 | tf_op jit(solution)/shard_map/all_to_all | solution.py:19
  78.5 0.0 reduce-scatter.2.cloned.1.call-done
  78.5 1.0 reshape_reduce_scatter.3
  79.6 21.7 %all_to_all.26.arrived_ref = f32[12,24,252]{2,1,0:T(8,128)S(1)} all-to-all(f32[12,24,252]{2,1,0:T(8,128)S(1)} %pad_maximum_fusion), channel_id=1, replica_groups=mesh['z'=12,'y'=8,'tp'=8] {'z'}, dimensions={0} | all-to-all | bytes 580608 | tf_op jit(solution)/shard_map/all_to_all | solution.py:287
  101.2 0.7 closing.1
  (28 shorter events, 0.2 us)
Async XLA Ops:
  7.2 14.8 %copy-start = (bf16[252,2016]{0,1:T(8,128)(2,1)S(1)}, bf16[252,2016]{0,1:T(8,128)(2,1)}, u32[]{:S(2)}) copy-start(bf16[252,2016]{0,1:T(8,128)(2,1)} %param.12) | copy-start | bytes 3048196
  7.2 17.9 %copy-start.1 = (bf16[512,2016]{0,1:T(8,128)(2,1)S(1)}, bf16[512,2016]{0,1:T(8,128)(2,1)}, u32[]{:S(2)}) copy-start(bf16[512,2016]{0,1:T(8,128)(2,1)} %param.13) | copy-start | bytes 6193156
  7.2 1.1 %copy-start.2 = (bf16[512,252]{1,0:T(8,128)(2,1)S(1)}, bf16[512,252]{1,0:T(8,128)(2,1)}, u32[]{:S(2)}) copy-start(bf16[512,252]{1,0:T(8,128)(2,1)} %conv_ref.5) | copy-start | bytes 774148
  8.3 16.8 %copy-start.8 = (bf16[252]{0:T(256)(128)(2,1)S(1)}, bf16[252]{0:T(256)(128)(2,1)}, u32[]{:S(2)}) copy-start(bf16[252]{0:T(256)(128)(2,1)} %param.11) | copy-start | bytes 1516
  8.3 16.8 %copy-start.3 = (bf16[512,252]{1,0:T(8,128)(2,1)S(1)}, bf16[512,252]{1,0:T(8,128)(2,1)}, u32[]{:S(2)}) copy-start(bf16[512,252]{1,0:T(8,128)(2,1)} %conv_ref.5) | copy-start | bytes 774148
  9.2 15.9 %all-to-all-start = ((f32[8,8,128]{2,1,0:T(8,128)}), f32[8,8,128]{2,1,0:T(8,128)S(1)}, u32[]{:S(2)}, u32[]{:S(2)}) async-start(f32[8,8,128]{2,1,0:T(8,128)} %statistics.1), calls=%async_computation | async-start | bytes 65536 | tf_op jit(solution)/shard_map/all_to_all | solution.py:258
  21.9 56.6 %reduce-scatter.2.cloned.1.call-start = ((), (), s32[]{:S(2)}) async-start(), calls=%async_computation.6 | async-start | bytes 2359296 | tf_op jit(solution)/shard_map/reduce_scatter | solution.py:262
  27.6 1.0 copy-start.4
  27.6 8.0 %slice-start = ((bf16[512,252]{1,0:T(8,128)(2,1)}), bf16[32,252]{1,0:T(8,128)(2,1)S(1)}, s32[]{:S(2)}) async-start(bf16[512,252]{1,0:T(8,128)(2,1)} %value_ref.3), calls=%async_computation.7 | async-start | bytes 32768 | tf_op jit(solution)/shard_map/slice | solution.py:265
  27.6 8.0 %slice-start.1 = ((bf16[512,252]{1,0:T(8,128)(2,1)}), bf16[32,252]{1,0:T(8,128)(2,1)S(1)}, s32[]{:S(2)}) async-start(bf16[512,252]{1,0:T(8,128)(2,1)} %gate_ref.3), calls=%async_computation.8 | async-start | bytes 32768 | tf_op jit(solution)/shard_map/slice | solution.py:265
  27.6 11.4 %copy-start.5 = (bf16[512,252]{1,0:T(8,128)(2,1)S(1)}, bf16[512,252]{1,0:T(8,128)(2,1)}, u32[]{:S(2)}) copy-start(bf16[512,252]{1,0:T(8,128)(2,1)} %value_ref.3) | copy-start | bytes 774148
  27.6 11.4 %copy-start.6 = (bf16[512,252]{1,0:T(8,128)(2,1)S(1)}, bf16[512,252]{1,0:T(8,128)(2,1)}, u32[]{:S(2)}) copy-start(bf16[512,252]{1,0:T(8,128)(2,1)} %gate_ref.3) | copy-start | bytes 774148
  27.7 32.3 %copy-start.7 = (bf16[31,252]{1,0:T(8,128)(2,1)S(1)}, bf16[31,252]{1,0:T(8,128)(2,1)}, u32[]{:S(2)}) copy-start(bf16[31,252]{1,0:T(8,128)(2,1)} %taps_ref.1) | copy-start | bytes 46876
  30.0 8.6 %all-to-all-start.1 = ((f32[8,8,128]{2,1,0:T(8,128)}), f32[8,8,128]{2,1,0:T(8,128)S(1)}, u32[]{:S(2)}, u32[]{:S(2)}) async-start(f32[8,8,128]{2,1,0:T(8,128)} %get-tuple-element.24), calls=%async_computation.1 | async-start | bytes 65536 | tf_op jit(solution)/shard_map/all_to_all | solution.py:258
  35.6 3.3 %collective-permute-start = (f32[32,252]{1,0:T(8,128)S(1)}, f32[32,252]{1,0:T(8,128)S(1)}, u32[]{:S(2)}, u32[]{:S(2)}) collective-permute-start(f32[32,252]{1,0:T(8,128)S(1)} %divide_multiply_fusion), channel_id=1, source_target_pairs={{0,8},{8,16},{16,24},{24,32},{32,40},{40,48},{48,56},{56,64},{64,7... | collective-permute-start | bytes 96776 | tf_op jit(solution)/shard_map/ppermute | solution.py:37
  41.8 22.6 %all-to-all-start.2 = ((f32[12,3,252]{2,1,0:T(4,128)}), f32[12,3,252]{2,1,0:T(4,128)S(1)}, u32[]{:S(2)}, u32[]{:S(2)}) async-start(f32[12,3,252]{2,1,0:T(4,128)} %reshape.58), calls=%async_computation.2 | async-start | bytes 98304 | tf_op jit(solution)/shard_map/all_to_all | solution.py:31
  53.6 6.4 %collective-permute-start.1 = (f32[30,252]{1,0:T(8,128)S(1)}, f32[30,252]{1,0:T(8,128)S(1)}, u32[]{:S(2)}, u32[]{:S(2)}) collective-permute-start(f32[30,252]{1,0:T(8,128)S(1)} %slice.32), channel_id=1, source_target_pairs={{8,0},{16,8},{24,16},{32,24},{40,32},{48,40},{56,48},{64,56},{72,6... | collective-permute-start | bytes 90728 | tf_op jit(solution)/shard_map/ppermute | solution.py:37
Sparse Core Ops, SparseCore 0:
  27.8 46.9 reduce-scatter.1

commit v5 on v1

--- a/solution.py
+++ b/solution.py
@@ -212,6 +212,31 @@
         compiler_params=pltpu.CompilerParams(vmem_limit_bytes=12 * 2**20),
         name="last_rows",
     )(conv_grad, ahead, value, gate, taps, *done)
+
+
+def closing_kernel(scale, arrived_ref, weight_out, tap_out):
+    each = weight_out.shape[0]
+    total = arrived_ref[0]
+    for z in range(1, arrived_ref.shape[0]):
+        total = total + arrived_ref[z]
+    weight_out[...] = total[:each] * scale
+    rows = arrived_ref.shape[1] - each
+    for z in range(arrived_ref.shape[0]):
+        at = z * rows
+        count = min(rows, tap_out.shape[0] - at)
+        if count > 0:
+            tap_out[at : at + count] = arrived_ref[z, each : each + count] * scale
+
+
+def closing(arrived, scale, each, tap_count):
+    width = arrived.shape[2]
+    return pl.pallas_call(
+        functools.partial(closing_kernel, scale),
+        out_shape=(jax.ShapeDtypeStruct((each, width), jnp.float32), jax.ShapeDtypeStruct((tap_count, width), jnp.float32)),
+        cost_estimate=pl.CostEstimate(flops=arrived.size, bytes_accessed=4 * arrived.size, transcendentals=0),
+        compiler_params=pltpu.CompilerParams(vmem_limit_bytes=4 * 2**20),
+        name="closing",
+    )(arrived)
 
 
 def local(proj_value, proj_gate, conv_saved, conv_taps, norm_gain, out_weight, cotangent):
@@ -249,8 +274,8 @@
     each = terms.shape[1]
     spread = jnp.broadcast_to(tap_part[None], (z_size, *tap_part.shape))
     arrived = lax.all_to_all(jnp.concatenate([terms, spread], axis=1), "z", 0, 0, tiled=True)
-    grad_out_weight = arrived[:, :each].sum(axis=0).T * grad_scale
-    grad_taps = arrived[:, each:].reshape(-1, arrived.shape[2])[:tap_count] * grad_scale
+    weight_rows, grad_taps = closing(arrived, grad_scale, each, tap_count)
+    grad_out_weight = weight_rows.T
     return (grad_value, grad_gate, grad_out_weight, grad_taps)
 
 

time: 108 us -> 107 us (level)
  other arithmetic: 1.72 us -> 0.46 us
    mul x2 -> x0, other arithmetic: 1.23 us -> none  [the longest x1 0.62 us: local(): arrived[:, each:].reshape(-1, arrived.shape[2])[:tap_count] * grad_scale]
where the time goes in v5:
time: 107 us
  blocking collectives  52.5 us (49%)
  starting transfers between devices  19.6 us (18%)
  between operations  14.2 us (13%)
  Pallas kernels  9.4 us (9%)
  waiting for transfers between devices  4.6 us (4%)
  local copies, waits for them, and re-layouts  3.15 us (3%)
  matrix products  3.13 us (3%)
    all_to_all x1, blocking collectives, scattered_sum(): return lax.all_to_all(padded, axes, 0, 0, tiled=True).sum(axis=0)  20.4 us
    all_to_all x1, blocking collectives, local(): lax.all_to_all(jnp.concatenate([terms, spread], axis=1), 'z', 0, 0, tiled...  18.8 us
    all_to_all x2, starting transfers between devices, local(): everyone = lambda x: lax.all_to_all(x, 'tp', 0, 0, tiled=True)  18.3 us
    all_to_all x1, blocking collectives, from_everyone(): lax.all_to_all(jnp.broadcast_to(x[None], (size, *x.shape)), axis, 0, 0, t...  13.4 us
    dot_general x1, matrix products, local(): lax.dot_general(cotangent, out_weight, (((1,), (1,)), ((), ())), preferre...  3.13 us
    all_to_all x2, waiting for transfers between devices, local(): everyone = lambda x: lax.all_to_all(x, 'tp', 0, 0, tiled=True)  3.01 us
    pallas_call x1, Pallas kernels, main_rows(): pl.pallas_call(main_rows_kernel, out_shape=(grad, grad, jax.ShapeDtypeStr...  2.91 us
    pallas_call x1, Pallas kernels, weight_grad(): pl.pallas_call(functools.partial(weight_grad_kernel, model_width, z_size)...  2.54 us
  transfers between devices with their start and end apart: 4, of which 2 were waited for; matrix products, arithmetic and copies ran while one was open for 3% of the time, Pallas kernels for 5%

profile of v5, /device:TPU:4, one launch (start us, length us, event | category | flops | bytes accessed | tf_op | source)
XLA Modules:
  0.0 107.0 jit_solution(10424750491725881194)
XLA Ops:
  7.2 0.0 copy-start
  7.2 0.0 copy-start.1
  7.2 0.0 copy-start.2
  7.2 1.1 %copy-done.2 = bf16[512,252]{1,0:T(8,128)(2,1)S(1)} copy-done((bf16[512,252]{1,0:T(8,128)(2,1)S(1)}, bf16[512,252]{1,0:T(8,128)(2,1)}, u32[]{:S(2)}) %copy-start.2) | copy-done | bytes 258072
  8.3 0.9 statistics.1
  9.2 12.8 %all-to-all-start = ((f32[8,8,128]{2,1,0:T(8,128)}), f32[8,8,128]{2,1,0:T(8,128)S(1)}, u32[]{:S(2)}, u32[]{:S(2)}) async-start(f32[8,8,128]{2,1,0:T(8,128)} %statistics.1), calls=%async_computation | async-start | bytes 65536 | tf_op jit(solution)/shard_map/all_to_all | solution.py:252
  21.9 0.0 reduce-scatter.2.cloned.1.call-start
  21.9 0.0 copy-done
  21.9 3.1 %fusion.2.act_grad_ref = f32[512,252]{1,0:T(8,128)} fusion(bf16[512,2016]{0,1:T(8,128)(2,1)} %param.13, bf16[252,2016]{0,1:T(8,128)(2,1)S(1)} %copy-done), kind=kOutput, calls=%fused_computation.8 | convolution fusion | flops 520224768 | bytes 3596544 | tf_op jit(solution)/shard_map/dot_general | solution.py:249
  25.1 0.0 copy-done.8
  25.1 0.0 all-to-all-done.shared_ref
  25.1 0.0 copy-done.1
  25.1 2.5 %weight_grad.1 = f32[8,252,252]{2,1,0:T(8,128)} custom-call(f32[8,8,128]{2,1,0:T(8,128)S(1)} %all-to-all-done.shared_ref, bf16[512,252]{1,0:T(8,128)(2,1)S(1)} %copy-done.3, bf16[1,252]{1,0:T(2,128)(2,1)S(1)} %broadcast_in_dim.6.gain_ref, bf16[2016,512]{1,0:T(8,128)(2,1)S(1)} %bitcast.18), custom_call_target="tpu_custom_call" | custom-call | flops 520224768 | bytes 4096512 | tf_op jit(solution)/shard_map/weight_grad/pallas_call | solution.py:115
  27.6 0.0 reduce-scatter.2.cloned.1.call-update
  27.7 1.0 copy-done.4
  28.7 1.4 %norm_grad.1 = (f32[512,252]{1,0:T(8,128)S(1)}, f32[8,8,128]{2,1,0:T(8,128)}) custom-call(f32[8,8,128]{2,1,0:T(8,128)S(1)} %all-to-all-done.shared_ref, bf16[512,252]{1,0:T(8,128)(2,1)S(1)} %copy-done.3, bf16[1,252]{1,0:T(2,128)(2,1)S(1)} %broadcast_in_dim.6.gain_ref, f32[512,252]{1,0:T(8,128)S(1)} %copy-done.4), custom_call_target="tpu_custom_call" | custom-call | flops 2580480 | bytes 1290240 | tf_op jit(solution)/shard_map/norm_grad/pallas_call | solution.py:87
  30.1 5.5 %all-to-all-start.1 = ((f32[8,8,128]{2,1,0:T(8,128)}), f32[8,8,128]{2,1,0:T(8,128)S(1)}, u32[]{:S(2)}, u32[]{:S(2)}) async-start(f32[8,8,128]{2,1,0:T(8,128)} %get-tuple-element.19), calls=%async_computation.1 | async-start | bytes 65536 | tf_op jit(solution)/shard_map/all_to_all | solution.py:252
  35.6 3.0 %all-to-all-done.1 = f32[8,8,128]{2,1,0:T(8,128)S(1)} async-done(((f32[8,8,128]{2,1,0:T(8,128)}), f32[8,8,128]{2,1,0:T(8,128)S(1)}, u32[]{:S(2)}, u32[]{:S(2)}) %all-to-all-start.1) | async-done | bytes 32800 | tf_op jit(solution)/shard_map/all_to_all | solution.py:252
  38.6 0.3 subtract_multiply_fusion.conv_grad_ref
  39.0 1.3 %collective-permute-start = (f32[30,252]{1,0:T(8,128)S(1)}, f32[30,252]{1,0:T(8,128)S(1)}, u32[]{:S(2)}, u32[]{:S(2)}) collective-permute-start(f32[30,252]{1,0:T(8,128)S(1)} %slice.24), channel_id=1, source_target_pairs={{8,0},{16,8},{24,16},{32,24},{40,32},{48,40},{56,48},{64,56},{72,6... | collective-permute-start | bytes 90728 | tf_op jit(solution)/shard_map/ppermute | solution.py:37
  40.3 0.0 copy-done.5
  40.3 0.0 copy-done.6
  40.3 0.0 copy-done.7
  40.3 2.9 %main_rows.1 = (bf16[512,252]{1,0:T(8,128)(2,1)S(1)}, bf16[512,252]{1,0:T(8,128)(2,1)S(1)}, f32[31,8,252]{2,1,0:T(8,128)S(1)}) custom-call(f32[512,252]{1,0:T(8,128)S(1)} %subtract_multiply_fusion.conv_grad_ref, bf16[512,252]{1,0:T(8,128)(2,1)S(1)} %copy-done.5, bf16[512,252]{1,0:T(8,128)(2,1)S(1)} %copy-done.6, bf16[31,252]{1,0:T(8,128)(2,1)S(1)} %copy-done.7), custom_call_target="tpu_custom_call" | custom-call | flops 15998976 | bytes 1548288 | tf_op jit(solution)/shard_map/main_rows/pallas_call | solution.py:195
  43.2 1.6 %collective-permute-done.ahead_ref = f32[30,252]{1,0:T(8,128)S(1)} collective-permute-done((f32[30,252]{1,0:T(8,128)S(1)}, f32[30,252]{1,0:T(8,128)S(1)}, u32[]{:S(2)}, u32[]{:S(2)}) %collective-permute-start) | collective-permute-done | bytes 30272 | tf_op jit(solution)/shard_map/ppermute | solution.py:37
  44.8 1.0 last_rows.1
  45.9 20.4 %all_to_all.25 = f32[12,3,252]{2,1,0:T(4,128)S(1)} all-to-all(f32[12,3,252]{2,1,0:T(4,128)S(1)} %reshape.58), channel_id=1, replica_groups=mesh['z'=12,'y'=8,'tp'=8] {'z'}, dimensions={0} | all-to-all | bytes 72576 | tf_op jit(solution)/shard_map/all_to_all | solution.py:31
  66.3 13.4 %all_to_all.26 = f32[8,3,252]{2,1,0:T(4,128)S(1)} all-to-all(f32[8,3,252]{2,1,0:T(4,128)S(1)} %broadcast_in_dim.7), channel_id=1, replica_groups=mesh['z'=12,'y'=8,'tp'=8] {'y'}, dimensions={0} | all-to-all | bytes 48384 | tf_op jit(solution)/shard_map/all_to_all | solution.py:19
  79.7 0.0 reduce-scatter.2.cloned.1.call-done
  79.7 1.0 reshape_reduce_scatter.3
  80.7 18.8 %all_to_all.27.arrived_ref = f32[12,24,252]{2,1,0:T(8,128)S(1)} all-to-all(f32[12,24,252]{2,1,0:T(8,128)S(1)} %pad_maximum_fusion), channel_id=1, replica_groups=mesh['z'=12,'y'=8,'tp'=8] {'z'}, dimensions={0} | all-to-all | bytes 580608 | tf_op jit(solution)/shard_map/all_to_all | solution.py:276
  99.5 0.7 closing.1
  (20 shorter events, 0.2 us)
Async XLA Ops:
  7.2 14.8 %copy-start = (bf16[252,2016]{0,1:T(8,128)(2,1)S(1)}, bf16[252,2016]{0,1:T(8,128)(2,1)}, u32[]{:S(2)}) copy-start(bf16[252,2016]{0,1:T(8,128)(2,1)} %param.12) | copy-start | bytes 3048196
  7.2 17.9 %copy-start.1 = (bf16[512,2016]{0,1:T(8,128)(2,1)S(1)}, bf16[512,2016]{0,1:T(8,128)(2,1)}, u32[]{:S(2)}) copy-start(bf16[512,2016]{0,1:T(8,128)(2,1)} %param.13) | copy-start | bytes 6193156
  7.2 1.1 %copy-start.2 = (bf16[512,252]{1,0:T(8,128)(2,1)S(1)}, bf16[512,252]{1,0:T(8,128)(2,1)}, u32[]{:S(2)}) copy-start(bf16[512,252]{1,0:T(8,128)(2,1)} %conv_ref.5) | copy-start | bytes 774148
  8.3 16.8 %copy-start.8 = (bf16[252]{0:T(256)(128)(2,1)S(1)}, bf16[252]{0:T(256)(128)(2,1)}, u32[]{:S(2)}) copy-start(bf16[252]{0:T(256)(128)(2,1)} %param.11) | copy-start | bytes 1516
  8.3 16.8 %copy-start.3 = (bf16[512,252]{1,0:T(8,128)(2,1)S(1)}, bf16[512,252]{1,0:T(8,128)(2,1)}, u32[]{:S(2)}) copy-start(bf16[512,252]{1,0:T(8,128)(2,1)} %conv_ref.5) | copy-start | bytes 774148
  9.2 15.9 %all-to-all-start = ((f32[8,8,128]{2,1,0:T(8,128)}), f32[8,8,128]{2,1,0:T(8,128)S(1)}, u32[]{:S(2)}, u32[]{:S(2)}) async-start(f32[8,8,128]{2,1,0:T(8,128)} %statistics.1), calls=%async_computation | async-start | bytes 65536 | tf_op jit(solution)/shard_map/all_to_all | solution.py:252
  21.9 57.8 %reduce-scatter.2.cloned.1.call-start = ((), (), s32[]{:S(2)}) async-start(), calls=%async_computation.6 | async-start | bytes 2359296 | tf_op jit(solution)/shard_map/reduce_scatter | solution.py:256
  27.6 1.0 copy-start.4
  27.6 12.7 %copy-start.5 = (bf16[512,252]{1,0:T(8,128)(2,1)S(1)}, bf16[512,252]{1,0:T(8,128)(2,1)}, u32[]{:S(2)}) copy-start(bf16[512,252]{1,0:T(8,128)(2,1)} %value_ref.3) | copy-start | bytes 774148
  27.6 12.7 %copy-start.6 = (bf16[512,252]{1,0:T(8,128)(2,1)S(1)}, bf16[512,252]{1,0:T(8,128)(2,1)}, u32[]{:S(2)}) copy-start(bf16[512,252]{1,0:T(8,128)(2,1)} %gate_ref.3) | copy-start | bytes 774148
  27.6 12.7 %copy-start.7 = (bf16[31,252]{1,0:T(8,128)(2,1)S(1)}, bf16[31,252]{1,0:T(8,128)(2,1)}, u32[]{:S(2)}) copy-start(bf16[31,252]{1,0:T(8,128)(2,1)} %taps_ref.3) | copy-start | bytes 46876
  30.1 8.6 %all-to-all-start.1 = ((f32[8,8,128]{2,1,0:T(8,128)}), f32[8,8,128]{2,1,0:T(8,128)S(1)}, u32[]{:S(2)}, u32[]{:S(2)}) async-start(f32[8,8,128]{2,1,0:T(8,128)} %get-tuple-element.19), calls=%async_computation.1 | async-start | bytes 65536 | tf_op jit(solution)/shard_map/all_to_all | solution.py:252
  39.0 5.8 %collective-permute-start = (f32[30,252]{1,0:T(8,128)S(1)}, f32[30,252]{1,0:T(8,128)S(1)}, u32[]{:S(2)}, u32[]{:S(2)}) collective-permute-start(f32[30,252]{1,0:T(8,128)S(1)} %slice.24), channel_id=1, source_target_pairs={{8,0},{16,8},{24,16},{32,24},{40,32},{48,40},{56,48},{64,56},{72,6... | collective-permute-start | bytes 90728 | tf_op jit(solution)/shard_map/ppermute | solution.py:37
Sparse Core Ops, SparseCore 0:
  27.8 46.5 reduce-scatter.1
